TPU v7x, 256 devices: a whole 4x4x8 slice. The times are simulated.
256 devices in a mesh: sp: 16 (over y, x), tp: 16 (over z, core).
Axes of the slice: x: 4, y: 4, z: 8, core: 2. Of those that a mesh axis runs over, the one named last changes fastest.
Arguments:
- tokens: bfloat16 [8192, 2048], P(('sp', 'tp')), may hold values from -6 to 6
- query_vectors: bfloat16 [8192, 2048], P('sp', 'tp'), may hold values from -8 to 8
- key_vectors: bfloat16 [8192, 2048], P('sp', 'tp'), may hold values from -8 to 8
- value_vectors: bfloat16 [8192, 2048], P('sp', 'tp'), may hold values from -24 to 24
- cum_gate: float32 [8192, 32], P('sp', 'tp'), may hold values from -1028 to 0, as said below
- out_weight: bfloat16 [2048, 2048], P('tp'), may hold values from -0.125 to 0.125
- norm_gain: float32 [2048], replicated, may hold values from 0.1 to 1.9
- gate_weight: bfloat16 [16, 2048, 7168], P('sp', None, 'tp'), may hold values from -0.125 to 0.125
- up_weight: bfloat16 [16, 2048, 7168], P('sp', None, 'tp'), may hold values from -0.125 to 0.125
- down_weight: bfloat16 [16, 7168, 2048], P('sp', 'tp'), may hold values from -0.0625 to 0.0625
- expert_ids: int32 [8192, 2], P(('sp', 'tp')), may hold values from 0 to 15, all different within a row; in each aligned block of 32 rows (0 to 31, 32 to 63, ...) at most 6 rows name the same one
- route_weights: float32 [8192, 2], P(('sp', 'tp')), may hold values from 0.2 to 1
Outputs:
- layer_output: bfloat16 [8192, 2048], P(('sp', 'tp'))
Inputs may be any that keep to these rules, and one draw needn't show every extreme that they name: `cum_gate`: along the positions each head's values never rise. `expert_ids`: within the rows of one device no expert is named by more than 6 rows, and in some devices' rows one expert is named by exactly 6; a row names 2 different experts.
All inputs are finite; a program needn't handle non-finite values.
Results may differ from a plain program's by a relative error of at most 0.014.
Values may be sent and summed in bfloat16 or wider, within the bound.
A program may use at most 128 MiB of HBM per device.

v0:
```python
import math

import jax
import jax.numpy as jnp
from jax import lax
from jax.sharding import PartitionSpec as P

NEG_LARGE = -1e30


def copy_for_each(shard, axis):
    peers = lax.axis_size(axis)
    return lax.all_to_all(
        jnp.broadcast_to(shard[None], (peers, *shard.shape)), axis, 0, 0, tiled=True
    )


def in_order(parts, dim):
    parts = jnp.moveaxis(parts, 0, dim)
    dims = parts.shape
    return parts.reshape(*dims[:dim], dims[dim] * dims[dim + 1], *dims[dim + 2 :])


def collect(shard, axis, dim):
    parts = copy_for_each(shard, axis)
    return in_order(parts, dim)


def sent_together(arrays, axis, dim, along):
    widths = [a.shape[along] for a in arrays]
    both = jnp.concatenate(arrays, axis=along)
    filled = lax.all_gather(both, axis, axis=dim, tiled=True)
    return tuple(jnp.split(filled, [sum(widths[:k]) for k in range(1, len(widths))], axis=along))


def shards(
    tokens,
    query_vectors,
    key_vectors,
    value_vectors,
    cum_gate,
    out_weight,
    norm_gain,
    gate_weight,
    up_weight,
    down_weight,
    expert_ids,
    route_weights,
):
    sp_count = lax.axis_size("sp")
    seg_rows = query_vectors.shape[0]
    heads_here = cum_gate.shape[1]
    head_width = query_vectors.shape[1] // heads_here
    score_scale = head_width ** (-0.5)
    offset = lax.axis_index("sp") * seg_rows
    last_query = offset + seg_rows - 1
    query_pos = offset + jnp.arange(seg_rows, dtype=jnp.int32)
    query_heads = query_vectors.reshape(seg_rows, heads_here, head_width)
    query_gate = cum_gate.T
    gate_rows = collect(cum_gate, "sp", 0)

    def attend_block(carried, key_block, value_block, block_start):
        running_peak, running_total, accumulated = carried
        row_count = key_block.shape[0]
        key_heads = key_block.reshape(row_count, heads_here, head_width)
        value_heads = value_block.reshape(row_count, heads_here, head_width)
        key_gate = lax.dynamic_slice_in_dim(gate_rows, block_start, row_count, 0).T
        scores = (
            jnp.einsum("qhd,khd->hqk", query_heads, key_heads, preferred_element_type=jnp.float32)
            * score_scale
        )
        scores = scores + query_gate[:, :, None] - key_gate[:, None, :]
        key_pos = block_start + jnp.arange(row_count, dtype=jnp.int32)
        visible = (key_pos[None, :] <= query_pos[:, None])[None]
        scores = jnp.where(visible, scores, NEG_LARGE)
        new_peak = jnp.maximum(running_peak, jnp.max(scores, axis=2))
        exponent = jnp.where(visible, jnp.exp(scores - new_peak[:, :, None]), 0.0)
        rescale = jnp.exp(running_peak - new_peak)
        running_total = running_total * rescale + jnp.sum(exponent, axis=2)
        weighted = jnp.einsum(
            "hqk,khd->hqd",
            exponent.astype(jnp.bfloat16),
            value_heads,
            preferred_element_type=jnp.float32,
        )
        accumulated = accumulated * rescale[:, :, None] + weighted
        return (new_peak, running_total, accumulated)

    start_state = (
        jnp.full((heads_here, seg_rows), NEG_LARGE, jnp.float32),
        jnp.zeros((heads_here, seg_rows), jnp.float32),
        jnp.zeros((heads_here, seg_rows, head_width), jnp.float32),
    )
    carried = start_state
    key_piece, value_piece = sent_together((key_vectors, value_vectors), "sp", 0, 1)
    row_count = key_piece.shape[0]
    block_rows = math.gcd(row_count, 1024)
    block_count = row_count // block_rows
    key_stack = key_piece.reshape(block_count, block_rows, key_piece.shape[1])
    value_stack = value_piece.reshape(block_count, block_rows, value_piece.shape[1])

    def step_block(state, inputs):
        key_block, value_block, block_index = inputs
        block_start = block_index * block_rows

        def take_block(inner):
            return attend_block(inner, key_block, value_block, block_start)

        def skip_block(inner):
            return inner

        return (lax.cond(block_start <= last_query, take_block, skip_block, state), None)

    carried, _ = lax.scan(
        step_block, carried, (key_stack, value_stack, jnp.arange(block_count, dtype=jnp.int32))
    )
    final_peak, final_total, accumulated = carried
    attended = (accumulated / final_total[:, :, None]).astype(jnp.bfloat16)
    attended = attended.transpose(1, 0, 2).reshape(seg_rows, heads_here * head_width)
    tok_dev = tokens.shape[0]
    model_width = tokens.shape[1]
    token_rows = lax.all_to_all(attended, "tp", split_axis=0, concat_axis=1, tiled=True)
    projected = jnp.dot(
        token_rows,
        lax.all_gather(out_weight, "tp", axis=0, tiled=True),
        preferred_element_type=jnp.float32,
    )
    stream_wide = (tokens.astype(jnp.float32) + projected).astype(jnp.bfloat16).astype(jnp.float32)
    inverse = lax.rsqrt(jnp.mean(stream_wide * stream_wide, axis=1, keepdims=True) + 1e-05)
    normed = (stream_wide * inverse * norm_gain[None, :]).astype(jnp.bfloat16)
    n_experts = gate_weight.shape[0] * sp_count
    top_count = expert_ids.shape[1]
    capacity = max(2, 3 * tok_dev * top_count // (2 * n_experts))
    flat_ids = expert_ids.reshape(-1)
    hits = (flat_ids[:, None] == jnp.arange(n_experts, dtype=jnp.int32)[None, :]).astype(jnp.int32)
    earlier = jnp.cumsum(hits, axis=0) - hits
    slot_index = flat_ids * capacity + jnp.sum(earlier * hits, axis=1)
    placement_map = (
        jnp.arange(n_experts * capacity, dtype=jnp.int32)[:, None] == slot_index[None, :]
    ).astype(jnp.bfloat16)
    repeated = jnp.repeat(normed, top_count, axis=0)
    dispatch = jnp.dot(placement_map, repeated, preferred_element_type=jnp.float32).astype(
        jnp.bfloat16
    )
    dispatch = dispatch.reshape(n_experts, capacity, model_width)
    arrived = lax.all_to_all(dispatch, "sp", split_axis=0, concat_axis=0, tiled=True)
    row_block = arrived.reshape(-1, model_width)
    rows_in = lax.all_gather(row_block, "tp", axis=0, tiled=True)
    gate_value = jnp.dot(rows_in, gate_weight[0], preferred_element_type=jnp.float32)
    up_value = jnp.dot(rows_in, up_weight[0], preferred_element_type=jnp.float32)
    hidden = (jax.nn.silu(gate_value) * up_value).astype(jnp.bfloat16)
    summed = lax.psum_scatter(
        jnp.dot(hidden, down_weight[0], preferred_element_type=jnp.float32).astype(jnp.bfloat16),
        "tp",
        scatter_dimension=0,
        tiled=True,
    )
    returned = summed.reshape(arrived.shape)
    back = lax.all_to_all(returned, "sp", split_axis=0, concat_axis=0, tiled=True)
    flat_back = back.reshape(n_experts * capacity, model_width)
    picked = flat_back[slot_index].astype(jnp.float32).reshape(tok_dev, top_count, model_width)
    mixture = jnp.sum(picked * route_weights[:, :, None], axis=1)
    return (stream_wide + mixture).astype(jnp.bfloat16)


def solution(mesh):
    in_specs = (
        P(("sp", "tp"), None),
        P("sp", "tp"),
        P("sp", "tp"),
        P("sp", "tp"),
        P("sp", "tp"),
        P("tp", None),
        P(),
        P("sp", None, "tp"),
        P("sp", None, "tp"),
        P("sp", "tp", None),
        P(("sp", "tp"), None),
        P(("sp", "tp"), None),
    )
    out_specs = P(("sp", "tp"), None)
    return jax.shard_map(shards, mesh=mesh, in_specs=in_specs, out_specs=out_specs, check_vma=False)
```

profile of v0, /device:TPU:2, one launch (start us, length us, event | category | flops | bytes accessed | tf_op | source)
XLA Modules:
  0.0 335.4 jit_solution(8175806650671181984)
XLA Ops:
  6.5 1.8 pad_maximum_fusion
  8.4 0.7 all-gather.6.cloned.1.call-update
  9.2 1.3 broadcast_in_dim.61
  10.5 7.5 %all-to-all-start = ((f32[16,512,2]{1,2,0:T(2,128)}), f32[16,512,2]{1,2,0:T(2,128)S(1)}, u32[]{:S(2)}, u32[]{:S(2)}) async-start(f32[16,512,2]{1,2,0:T(2,128)} %broadcast_in_dim.61), calls=%async_computation | async-start | bytes 131072 | tf_op jit(solution)/shard_map/all_to_all | solution.py:13
  18.0 1.0 copy.28
  19.0 0.8 copy.33
  20.0 49.1 %all-gather.4.cloned.1.call-done = bf16[8192,256]{1,0:T(8,128)(2,1)} async-done(((bf16[512,256]{1,0:T(8,128)(2,1)}), bf16[8192,256]{1,0:T(8,128)(2,1)}) %all-gather.4.cloned.1.call-update) | async-done | bytes 4194320 | tf_op jit(solution)/shard_map/all_gather | solution.py:32
  69.2 4.4 %fusion.30 = (bf16[8192,128]{1,0:T(8,128)(2,1)}, bf16[8192,128]{1,0:T(8,128)(2,1)}) fusion(bf16[8192,256]{1,0:T(8,128)(2,1)} %all-gather.4.cloned.1.call-done), kind=kLoop, calls=%fused_computation.54 | loop fusion | bytes 8388608 | tf_op jit(solution)/shard_map/split | solution.py:33
  73.6 3.9 %copy.29 = bf16[8,1024,128]{1,2,0:T(8,128)(2,1)} copy(bf16[8,1024,128]{2,1,0:T(8,128)(2,1)} %bitcast.60) | data formatting | bytes 4194304
  77.5 3.9 %copy.30 = bf16[8,1024,128]{1,2,0:T(8,128)(2,1)} copy(bf16[8,1024,128]{2,1,0:T(8,128)(2,1)} %bitcast.59) | data formatting | bytes 4194304
  81.5 16.5 %while.15 = (s32[]{:T(128)}, f32[2,512]{1,0:T(2,128)S(1)}, f32[2,512]{1,0:T(2,128)S(1)}, f32[2,512,64]{1,2,0:T(8,128)S(1)}, s32[8]{0:T(128)S(1)}, /*index=5*/s32...) while((s32[]{:T(128)}, f32[2,512]{1,0:T(2,128)S(1)}, ...), condition=%wide.region_5.6_spmd.clone, body=%wide.region_0.5_spmd.clone.sunk | while | flops 289017344 | bytes 17043828 | solution.py:114
  82.8 6.2 %conditional.3 = ((f32[2,512]{1,0:T(2,128)S(1)}, f32[2,512]{1,0:T(2,128)S(1)}, f32[2,512,64]{1,2,0:T(8,128)S(1)})) conditional(s32[]{:T(128)} %convert_element_type.83, (f32[2,512]{1,0:T(2,128)S(1)}, f32[2,512]{1,0:T(2,128)S(1)}, f32[2,512,64]{1,2,0:T(8,128)S(1)}) %tuple.43, (s32[]{:T(128)}, s32[]{:T(128)}, bf16[8,1024,128]{1,2,0:T(8,128)(2,1)}, ...), branch_computations={%region_1.1_spmd, %region_2.4_spmd} | conditional | flops 289017344 | bytes 17041490 | solution.py:112
  83.3 1.1 constant_dynamic-slice_fusion
  84.3 1.4 fusion.4
  85.7 1.5 fusion.3
  87.2 1.7 fusion.8
  98.2 0.8 all_to_all.24
  99.0 7.1 %all-to-all-start.1 = ((bf16[16,32,128]{2,1,0:T(8,128)(2,1)}), bf16[16,32,128]{2,1,0:T(8,128)(2,1)S(1)}, u32[]{:S(2)}, u32[]{:S(2)}) async-start(bf16[16,32,128]{2,1,0:T(8,128)(2,1)} %all_to_all.24), calls=%async_computation.1 | async-start | bytes 262144 | tf_op jit(solution)/shard_map/all_to_all | solution.py:122
  106.4 10.4 %all-to-all-done.1 = bf16[16,32,128]{2,1,0:T(8,128)(2,1)S(1)} async-done(((bf16[16,32,128]{2,1,0:T(8,128)(2,1)}), bf16[16,32,128]{2,1,0:T(8,128)(2,1)S(1)}, u32[]{:S(2)}, u32[]{:S(2)}) %all-to-all-start.1) | async-done | bytes 131104 | tf_op jit(solution)/shard_map/all_to_all | solution.py:122
  116.8 12.6 %all-gather.6.cloned.1.call-done = bf16[2048,2048]{1,0:T(8,128)(2,1)} async-done(((bf16[128,2048]{1,0:T(8,128)(2,1)}), bf16[2048,2048]{1,0:T(8,128)(2,1)}) %all-gather.6.cloned.1.call-update) | async-done | bytes 8388624 | tf_op jit(solution)/shard_map/all_gather | solution.py:125
  129.4 5.0 %multiply_reduce_fusion.1 = (f32[32]{0:T(128)S(1)}, f32[32,2048]{1,0:T(8,128)S(1)}) fusion(bf16[2048,2048]{1,0:T(8,128)(2,1)} %all-gather.6.cloned.1.call-done, bf16[32,2048]{1,0:T(8,128)(2,1)S(1)} %copy-done.2, bf16[16,32,128]{2,1,0:T(8,128)(2,1)S(1)} %all-to-all-done.1), kind=kOutput, calls=%fused_computation.36 | convolution fusion | flops 268828640 | bytes 8913024 | tf_op jit(solution)/shard_map/dot_general | solution.py:123
  135.2 44.9 %all_to_all.34 = bf16[16,6,2048]{2,1,0:T(8,128)(2,1)S(1)} all-to-all(bf16[16,6,2048]{2,1,0:T(8,128)(2,1)S(1)} %reshape.145), channel_id=1, replica_groups=mesh['sp'=16,'tp'=16] {'sp'}, dimensions={0} | all-to-all | bytes 786432 | tf_op jit(solution)/shard_map/all_to_all | solution.py:146
  180.1 0.9 reshape.146
  181.3 40.0 %all-gather.8.cloned.1.call-done = bf16[1536,2048]{1,0:T(8,128)(2,1)} async-done(((bf16[96,2048]{1,0:T(8,128)(2,1)}), bf16[1536,2048]{1,0:T(8,128)(2,1)}) %all-gather.8.cloned.1.call-update) | async-done | bytes 6291472 | tf_op jit(solution)/shard_map/all_gather | solution.py:148
  221.2 7.9 %fusion.19 = f32[1536,448]{0,1:T(8,128)} fusion(bf16[1536,2048]{1,0:T(8,128)(2,1)} %all-gather.8.cloned.1.call-done, bf16[1,2048,448]{1,2,0:T(8,128)(2,1)} %param.23), kind=kOutput, calls=%fused_computation.30 | convolution fusion | flops 2818572288 | bytes 10878976 | tf_op jit(solution)/shard_map/dot_general | solution.py:149
  229.1 13.2 %convolution_convert_fusion = bf16[1536,2048]{1,0:T(8,128)(2,1)} fusion(bf16[1,448,2048]{2,1,0:T(8,128)(2,1)S(1)} %copy-done, bf16[1536,2048]{1,0:T(8,128)(2,1)} %all-gather.8.cloned.1.call-done, f32[1536,448]{0,1:T(8,128)} %fusion.19, bf16[1,2048,448]{1,2,0:T(8,128)(2,1)} %param.24), kind=kOutput, calls=%fused_computation.21 | convolution fusion | flops 5644419072 | bytes 19005440 | tf_op jit(solution)/shard_map/dot_general | solution.py:153
  242.3 65.9 %reduce-scatter.2.cloned.1.call-done = bf16[96,2048]{1,0:T(8,128)(2,1)} async-done(((bf16[1536,2048]{1,0:T(8,128)(2,1)}), bf16[96,2048]{1,0:T(8,128)(2,1)}) %reduce-scatter.2.cloned.1.call-update) | async-done | bytes 393232 | tf_op jit(solution)/shard_map/reduce_scatter | solution.py:152
  308.2 1.9 reshape.147
  310.2 7.2 %all-to-all-start.3 = ((bf16[16,6,2048]{2,1,0:T(8,128)(2,1)}), bf16[16,6,2048]{2,1,0:T(8,128)(2,1)S(1)}, u32[]{:S(2)}, u32[]{:S(2)}) async-start(bf16[16,6,2048]{2,1,0:T(8,128)(2,1)} %reshape.147), calls=%async_computation.4 | async-start | bytes 1048576 | tf_op jit(solution)/shard_map/all_to_all | solution.py:159
  317.7 8.5 %all-to-all-done.3 = bf16[16,6,2048]{2,1,0:T(8,128)(2,1)S(1)} async-done(((bf16[16,6,2048]{2,1,0:T(8,128)(2,1)}), bf16[16,6,2048]{2,1,0:T(8,128)(2,1)S(1)}, u32[]{:S(2)}, u32[]{:S(2)}) %all-to-all-start.3) | async-done | bytes 393248 | tf_op jit(solution)/shard_map/all_to_all | solution.py:159
  326.3 0.7 gather_fusion
  327.4 0.7 multiply_reduce_fusion
  (76 shorter events, 8.5 us)
Async XLA Ops:
  6.5 222.6 %copy-start = (bf16[1,448,2048]{2,1,0:T(8,128)(2,1)S(1)}, bf16[1,448,2048]{2,1,0:T(8,128)(2,1)}, u32[]{:S(2)}) copy-start(bf16[1,448,2048]{2,1,0:T(8,128)(2,1)} %param.25) | copy-start | bytes 5505028
  6.5 62.6 %all-gather.4.cloned.1.call-start = ((), (), s32[]{:S(2)}) async-start(), calls=%async_computation.5 | async-start | bytes 4456448 | tf_op jit(solution)/shard_map/all_gather | solution.py:32
  8.4 121.0 %all-gather.6.cloned.1.call-start = ((), (), s32[]{:S(2)}) async-start(), calls=%async_computation.6 | async-start | bytes 8912896 | tf_op jit(solution)/shard_map/all_gather | solution.py:125
  10.5 70.9 %all-to-all-start = ((f32[16,512,2]{1,2,0:T(2,128)}), f32[16,512,2]{1,2,0:T(2,128)S(1)}, u32[]{:S(2)}, u32[]{:S(2)}) async-start(f32[16,512,2]{1,2,0:T(2,128)} %broadcast_in_dim.61), calls=%async_computation | async-start | bytes 131072 | tf_op jit(solution)/shard_map/all_to_all | solution.py:13
  73.6 7.9 %copy-start.1 = (f32[512,2]{0,1:T(2,128)S(1)}, f32[512,2]{0,1:T(2,128)}, u32[]{:S(2)}) copy-start(f32[512,2]{0,1:T(2,128)} %param.20) | copy-start | bytes 12292
  81.5 47.9 %copy-start.2 = (bf16[32,2048]{1,0:T(8,128)(2,1)S(1)}, bf16[32,2048]{1,0:T(8,128)(2,1)}, u32[]{:S(2)}) copy-start(bf16[32,2048]{1,0:T(8,128)(2,1)} %param.16) | copy-start | bytes 393220
  99.0 17.7 %all-to-all-start.1 = ((bf16[16,32,128]{2,1,0:T(8,128)(2,1)}), bf16[16,32,128]{2,1,0:T(8,128)(2,1)S(1)}, u32[]{:S(2)}, u32[]{:S(2)}) async-start(bf16[16,32,128]{2,1,0:T(8,128)(2,1)} %all_to_all.24), calls=%async_computation.1 | async-start | bytes 262144 | tf_op jit(solution)/shard_map/all_to_all | solution.py:122
  106.1 115.1 %all-gather.8.cloned.1.call-start = ((), (), s32[]{:S(2)}) async-start(), calls=%async_computation.7 | async-start | bytes 6684672 | tf_op jit(solution)/shard_map/all_gather | solution.py:148
  106.4 28.1 %copy-start.3 = (f32[2048]{0:T(1024)S(1)}, f32[2048]{0:T(1024)}, u32[]{:S(2)}) copy-start(f32[2048]{0:T(1024)} %param.22) | copy-start | bytes 24580
  181.1 127.2 %reduce-scatter.2.cloned.1.call-start = ((), (), s32[]{:S(2)}) async-start(), calls=%async_computation.8 | async-start | bytes 6684672 | tf_op jit(solution)/shard_map/reduce_scatter | solution.py:152
  242.3 75.1 %copy-start.4 = (s32[32,2]{0,1:T(2,128)S(1)}, s32[32,2]{0,1:T(2,128)}, u32[]{:S(2)}) copy-start(s32[32,2]{0,1:T(2,128)} %param.26) | copy-start | bytes 772
  242.3 75.3 %copy-start.5 = (f32[32,2]{0,1:T(2,128)S(1)}, f32[32,2]{0,1:T(2,128)}, u32[]{:S(2)}) copy-start(f32[32,2]{0,1:T(2,128)} %param.27) | copy-start | bytes 772
  310.2 16.0 %all-to-all-start.3 = ((bf16[16,6,2048]{2,1,0:T(8,128)(2,1)}), bf16[16,6,2048]{2,1,0:T(8,128)(2,1)S(1)}, u32[]{:S(2)}, u32[]{:S(2)}) async-start(bf16[16,6,2048]{2,1,0:T(8,128)(2,1)} %reshape.147), calls=%async_computation.4 | async-start | bytes 1048576 | tf_op jit(solution)/shard_map/all_to_all | solution.py:159
Sparse Core Ops, SparseCore 0:
  9.8 59.3 all-gather.3
  71.0 58.3 all-gather.5
  181.2 40.0 all-gather.7
  242.5 65.7 reduce-scatter.1
where the time goes:
time: 336 us; the launch traced here: 335 us
  waiting for transfers between devices  187 us (56%)
  blocking collectives  44.9 us (13%)
  matrix products  29.4 us (9%)
  local copies, waits for them, and re-layouts  27.1 us (8%)
  starting transfers between devices  22.1 us (7%)
  between operations  13.3 us (4%)
  loops' own time  5.68 us (2%)
  other arithmetic  5.62 us (2%)
    reduce_scatter x1, waiting for transfers between devices, shards(): lax.psum_scatter(jnp.dot(hidden, down_weight[0], preferred_element_type=j...  65.9 us
    all_gather x1, waiting for transfers between devices, sent_together(): filled = lax.all_gather(both, axis, axis=dim, tiled=True)  49.1 us
    all_to_all x1, blocking collectives, shards(): lax.all_to_all(dispatch, 'sp', split_axis=0, concat_axis=0, tiled=True)  44.9 us
    all_gather x1, waiting for transfers between devices, shards(): rows_in = lax.all_gather(row_block, 'tp', axis=0, tiled=True)  40 us
    dot_general x1, matrix products, shards(): jnp.dot(hidden, down_weight[0], preferred_element_type=jnp.float32)  13.2 us
    all_gather x1, waiting for transfers between devices, shards(): lax.all_gather(out_weight, 'tp', axis=0, tiled=True)  12.6 us
    all_to_all x1, waiting for transfers between devices, shards(): lax.all_to_all(attended, 'tp', split_axis=0, concat_axis=1, tiled=True)  10.4 us
    unnamed x17, local copies, waits for them, and re-layouts  9.73 us
  transfers between devices with their start and end apart: 7, of which 6 were waited for; matrix products, arithmetic and copies ran while one was open for 8% of the time, Pallas kernels for 0%

commit v1 on v0

v1 whole, which is shorter than its diff:
```python
import functools
import math

import jax
import jax.numpy as jnp
from jax import lax
from jax.experimental import pallas as pl
from jax.experimental.pallas import tpu as pltpu
from jax.sharding import PartitionSpec as P

NEG_LARGE = -1e30
MESH = pl.DeviceIdType.MESH


def attention_kernel(
    n,
    n_tp,
    tok_dev,
    coef,
    q_ref,
    kv_ref,
    bias_ref,
    out_ref,
    qraw,
    qbuf,
    kvbuf,
    bbuf,
    peak,
    total,
    acc,
    obuf,
    rbuf,
    kv_send,
    kv_recv,
    b_send,
    b_recv,
    q_send,
    q_recv,
    o_send,
    o_recv,
):
    me = lax.axis_index("sp")
    mt = lax.axis_index("tp")
    head = lax.rem(me, 2)
    pair = lax.div(me, 2)
    rows = q_ref.shape[0]
    width = q_ref.shape[1]
    half = width // 2
    last = n - 1 - pair

    def kv_copy(r):
        hr = lax.rem(r, 2)
        return (
            pltpu.make_async_remote_copy(
                src_ref=kv_ref.at[hr],
                dst_ref=kvbuf.at[me],
                send_sem=kv_send.at[r],
                recv_sem=kv_recv.at[me],
                device_id=(r, mt),
                device_id_type=MESH,
            ),
            pltpu.make_async_remote_copy(
                src_ref=bias_ref.at[hr],
                dst_ref=bbuf.at[me],
                send_sem=b_send.at[r],
                recv_sem=b_recv.at[me],
                device_id=(r, mt),
                device_id_type=MESH,
            ),
        )

    q_slot = jnp.where(me < n // 2, 0, 1)
    q_target = 2 * jnp.minimum(me, n - 1 - me)

    def q_copy(h):
        return pltpu.make_async_remote_copy(
            src_ref=q_ref,
            dst_ref=qraw.at[q_slot],
            send_sem=q_send.at[h],
            recv_sem=q_recv.at[q_slot],
            device_id=(q_target + h, mt),
            device_id_type=MESH,
        )

    def q_local():
        return pltpu.make_async_copy(q_ref, qraw.at[q_slot], q_recv.at[q_slot])

    for h in range(2):

        @pl.when(q_target + h != me)
        def _():
            q_copy(h).start()

        @pl.when(q_target + h == me)
        def _():
            q_local().start()

    local_kv = pltpu.make_async_copy(kv_ref.at[head], kvbuf.at[me], kv_recv.at[me])
    local_b = pltpu.make_async_copy(bias_ref.at[head], bbuf.at[me], b_recv.at[me])

    @pl.when(me <= last)
    def _():
        local_kv.start()
        local_b.start()

    def send_body(k, c):
        r = lax.rem(me + k, n)

        @pl.when(me <= n - 1 - lax.div(r, 2))
        def _():
            ck, cb = kv_copy(r)
            cb.start()
            ck.start()

        return c

    lax.fori_loop(1, n, send_body, 0)

    lane = lax.broadcasted_iota(jnp.int32, (rows, width), 1)
    mine = (lane >= half) == (head == 0)
    for slot in range(2):
        pltpu.make_async_copy(q_ref, qraw.at[slot], q_recv.at[slot]).wait()
        qbuf[slot] = jnp.where(mine, qraw[slot].astype(jnp.float32), 0.0).astype(jnp.bfloat16)
    peak[...] = jnp.full(peak.shape, NEG_LARGE, jnp.float32)
    total[...] = jnp.zeros(total.shape, jnp.float32)
    acc[...] = jnp.zeros(acc.shape, jnp.float32)

    sub = min(256, rows)

    def tile(slot, j, diagonal):
        kv = kvbuf[j]
        bias = bbuf[j]
        for i in range(rows // sub):
            rs = pl.ds(i * sub, sub)
            s = lax.dot_general(
                qbuf[slot, rs, :], kv, (((1,), (1,)), ((), ())), preferred_element_type=jnp.float32
            )
            s = s * coef + bias
            if diagonal:
                qp = lax.broadcasted_iota(jnp.int32, s.shape, 0) + i * sub
                kp = lax.broadcasted_iota(jnp.int32, s.shape, 1)
                s = jnp.where(kp <= qp, s, NEG_LARGE)
            old = peak[slot, rs, :]
            new = jnp.maximum(old, jnp.max(s, axis=1, keepdims=True))
            e = jnp.exp2(s - new)
            alpha = jnp.exp2(old - new)
            total[slot, rs, :] = total[slot, rs, :] * alpha + jnp.sum(e, axis=1, keepdims=True)
            acc[slot, rs, :] = acc[slot, rs, :] * alpha + jnp.dot(
                e.astype(jnp.bfloat16), kv, preferred_element_type=jnp.float32
            )
            peak[slot, rs, :] = new

    def compute_body(k, c):
        j = lax.rem(me - k + n, n)

        @pl.when(j <= last)
        def _():
            pltpu.make_async_copy(kv_ref.at[0], kvbuf.at[j], kv_recv.at[j]).wait()
            pltpu.make_async_copy(bias_ref.at[0], bbuf.at[j], b_recv.at[j]).wait()

            @pl.when(j == last)
            def _():
                tile(1, j, True)

            @pl.when(j < last)
            def _():
                tile(1, j, False)

            @pl.when(j == pair)
            def _():
                tile(0, j, True)

            @pl.when(j < pair)
            def _():
                tile(0, j, False)

        return c

    lax.fori_loop(0, n, compute_body, 0)

    for slot in range(2):
        obuf[slot] = (acc[slot] / total[slot]).astype(jnp.bfloat16)

    def o_copy(slot, t):
        chunk = jnp.where(slot == 0, pair, last)
        return pltpu.make_async_remote_copy(
            src_ref=obuf.at[slot, pl.ds(t * tok_dev, tok_dev)],
            dst_ref=rbuf.at[mt, head],
            send_sem=o_send.at[slot, t],
            recv_sem=o_recv,
            device_id=(chunk, t),
            device_id_type=MESH,
        )

    def o_self(slot, t):
        chunk = jnp.where(slot == 0, pair, last)
        return jnp.logical_and(chunk == me, t == mt)

    def o_body(k, c):
        slot = lax.div(k, n_tp)
        t = lax.rem(mt + lax.rem(k, n_tp), n_tp)

        @pl.when(jnp.logical_not(o_self(slot, t)))
        def _():
            o_copy(slot, t).start()

        @pl.when(o_self(slot, t))
        def _():
            pltpu.make_async_copy(
                obuf.at[slot, pl.ds(t * tok_dev, tok_dev)], rbuf.at[mt, head], o_recv
            ).start()

        return c

    lax.fori_loop(0, 2 * n_tp, o_body, 0)

    pltpu.make_async_copy(rbuf, rbuf, o_recv).wait()
    lane32 = lax.broadcasted_iota(jnp.int32, (tok_dev, width), 1)
    for t in range(n_tp):
        out_ref[:, t * width : (t + 1) * width] = jnp.where(
            lane32 < half, rbuf[t, 0].astype(jnp.float32), rbuf[t, 1].astype(jnp.float32)
        ).astype(jnp.bfloat16)

    for h in range(2):

        @pl.when(q_target + h != me)
        def _():
            q_copy(h).wait_send()

    def drain_body(k, c):
        r = lax.rem(me + k, n)

        @pl.when(me <= n - 1 - lax.div(r, 2))
        def _():
            ck, cb = kv_copy(r)
            cb.wait_send()
            ck.wait_send()

        return c

    lax.fori_loop(1, n, drain_body, 0)

    def o_drain(k, c):
        slot = lax.div(k, n_tp)
        t = lax.rem(mt + lax.rem(k, n_tp), n_tp)

        @pl.when(jnp.logical_not(o_self(slot, t)))
        def _():
            o_copy(slot, t).wait_send()

        return c

    lax.fori_loop(0, 2 * n_tp, o_drain, 0)


def attention(query_vectors, key_vectors, value_vectors, cum_gate, tok_dev):
    n = lax.axis_size("sp")
    n_tp = lax.axis_size("tp")
    rows, width = query_vectors.shape
    half = width // 2
    coef = half ** (-0.5) * math.log2(math.e)
    q_swapped = jnp.concatenate([query_vectors[:, half:], query_vectors[:, :half]], axis=1)
    kv = jnp.stack(
        [
            jnp.concatenate([value_vectors[:, :half], key_vectors[:, :half]], axis=1),
            jnp.concatenate([key_vectors[:, half:], value_vectors[:, half:]], axis=1),
        ]
    )
    bias = (cum_gate * (-math.log2(math.e))).T[:, None, :]
    vmem = pl.BlockSpec(memory_space=pltpu.VMEM)
    tiles = n + 1
    return pl.pallas_call(
        functools.partial(attention_kernel, n, n_tp, tok_dev, coef),
        out_shape=jax.ShapeDtypeStruct((tok_dev, n_tp * width), jnp.bfloat16),
        in_specs=[vmem] * 3,
        out_specs=vmem,
        scratch_shapes=[
            pltpu.VMEM((2, rows, width), jnp.bfloat16),
            pltpu.VMEM((2, rows, width), jnp.bfloat16),
            pltpu.VMEM((n, rows, width), jnp.bfloat16),
            pltpu.VMEM((n, 1, rows), jnp.float32),
            pltpu.VMEM((2, rows, 1), jnp.float32),
            pltpu.VMEM((2, rows, 1), jnp.float32),
            pltpu.VMEM((2, rows, width), jnp.float32),
            pltpu.VMEM((2, rows, width), jnp.bfloat16),
            pltpu.VMEM((n_tp, 2, tok_dev, width), jnp.bfloat16),
            pltpu.SemaphoreType.DMA((n,)),
            pltpu.SemaphoreType.DMA((n,)),
            pltpu.SemaphoreType.DMA((n,)),
            pltpu.SemaphoreType.DMA((n,)),
            pltpu.SemaphoreType.DMA((2,)),
            pltpu.SemaphoreType.DMA((2,)),
            pltpu.SemaphoreType.DMA((2, n_tp)),
            pltpu.SemaphoreType.DMA,
        ],
        compiler_params=pltpu.CompilerParams(has_side_effects=True),
        cost_estimate=pl.CostEstimate(
            flops=tiles * rows * rows * width * 4 * 8,
            bytes_accessed=4 << 20,
            transcendentals=tiles * rows * rows,
        ),
        name="attention",
    )(q_swapped, kv, bias)


def shards(
    tokens,
    query_vectors,
    key_vectors,
    value_vectors,
    cum_gate,
    out_weight,
    norm_gain,
    gate_weight,
    up_weight,
    down_weight,
    expert_ids,
    route_weights,
):
    sp_count = lax.axis_size("sp")
    tok_dev = tokens.shape[0]
    model_width = tokens.shape[1]
    token_rows = attention(query_vectors, key_vectors, value_vectors, cum_gate, tok_dev)
    projected = jnp.dot(
        token_rows,
        lax.all_gather(out_weight, "tp", axis=0, tiled=True),
        preferred_element_type=jnp.float32,
    )
    stream_wide = (tokens.astype(jnp.float32) + projected).astype(jnp.bfloat16).astype(jnp.float32)
    inverse = lax.rsqrt(jnp.mean(stream_wide * stream_wide, axis=1, keepdims=True) + 1e-05)
    normed = (stream_wide * inverse * norm_gain[None, :]).astype(jnp.bfloat16)
    n_experts = gate_weight.shape[0] * sp_count
    top_count = expert_ids.shape[1]
    capacity = max(2, 3 * tok_dev * top_count // (2 * n_experts))
    flat_ids = expert_ids.reshape(-1)
    hits = (flat_ids[:, None] == jnp.arange(n_experts, dtype=jnp.int32)[None, :]).astype(jnp.int32)
    earlier = jnp.cumsum(hits, axis=0) - hits
    slot_index = flat_ids * capacity + jnp.sum(earlier * hits, axis=1)
    placement_map = (
        jnp.arange(n_experts * capacity, dtype=jnp.int32)[:, None] == slot_index[None, :]
    ).astype(jnp.bfloat16)
    repeated = jnp.repeat(normed, top_count, axis=0)
    dispatch = jnp.dot(placement_map, repeated, preferred_element_type=jnp.float32).astype(
        jnp.bfloat16
    )
    dispatch = dispatch.reshape(n_experts, capacity, model_width)
    arrived = lax.all_to_all(dispatch, "sp", split_axis=0, concat_axis=0, tiled=True)
    row_block = arrived.reshape(-1, model_width)
    rows_in = lax.all_gather(row_block, "tp", axis=0, tiled=True)
    gate_value = jnp.dot(rows_in, gate_weight[0], preferred_element_type=jnp.float32)
    up_value = jnp.dot(rows_in, up_weight[0], preferred_element_type=jnp.float32)
    hidden = (jax.nn.silu(gate_value) * up_value).astype(jnp.bfloat16)
    summed = lax.psum_scatter(
        jnp.dot(hidden, down_weight[0], preferred_element_type=jnp.float32).astype(jnp.bfloat16),
        "tp",
        scatter_dimension=0,
        tiled=True,
    )
    returned = summed.reshape(arrived.shape)
    back = lax.all_to_all(returned, "sp", split_axis=0, concat_axis=0, tiled=True)
    flat_back = back.reshape(n_experts * capacity, model_width)
    picked = flat_back[slot_index].astype(jnp.float32).reshape(tok_dev, top_count, model_width)
    mixture = jnp.sum(picked * route_weights[:, :, None], axis=1)
    return (stream_wide + mixture).astype(jnp.bfloat16)


def solution(mesh):
    in_specs = (
        P(("sp", "tp"), None),
        P("sp", "tp"),
        P("sp", "tp"),
        P("sp", "tp"),
        P("sp", "tp"),
        P("tp", None),
        P(),
        P("sp", None, "tp"),
        P("sp", None, "tp"),
        P("sp", "tp", None),
        P(("sp", "tp"), None),
        P(("sp", "tp"), None),
    )
    out_specs = P(("sp", "tp"), None)
    return jax.shard_map(shards, mesh=mesh, in_specs=in_specs, out_specs=out_specs, check_vma=False)
```

time: 336 us -> 264 us (0.79)
  waiting for transfers between devices: 187 us -> 115 us
  Pallas kernels: 0 us -> 65.9 us
  blocking collectives: 44.9 us -> 22.3 us
  local copies, waits for them, and re-layouts: 27.1 us -> 9.4 us
  starting transfers between devices: 22.1 us -> 7.56 us
  loops' own time: 5.68 us -> 0 us
    pallas_call x0 -> x1, Pallas kernels: none -> 65.9 us  [attention(): pl.pallas_call(functools.partial(attention_kernel, n, n_tp, tok_dev, coef...]
    all_gather x1 -> x0, waiting for transfers between devices: 49.1 us -> none  [sent_together(): filled = lax.all_gather(both, axis, axis=dim, tiled=True)]
    all_to_all x1, blocking collectives: 44.9 us -> 22.3 us  [shards(): lax.all_to_all(dispatch, 'sp', split_axis=0, concat_axis=0, tiled=True)]
    all_to_all x2 -> x0, starting transfers between devices: 14.6 us -> none  [the longest x1 7.48 us: copy_for_each(): lax.all_to_all(jnp.broadcast_to(shard[None], (peers, *shard.shape)), axis...]
    all_gather x1, waiting for transfers between devices: 12.6 us -> 0.02 us  [shards(): lax.all_gather(out_weight, 'tp', axis=0, tiled=True)]
    all_to_all x2 -> x0, waiting for transfers between devices: 10.4 us -> none  [the longest x1 10.4 us: shards(): lax.all_to_all(attended, 'tp', split_axis=0, concat_axis=1, tiled=True)]
    unnamed x17 -> x12, local copies, waits for them, and re-layouts: 9.73 us -> 0.87 us
    dynamic_slice x9 -> x0, local copies, waits for them, and re-layouts: 5.77 us -> none  [shards(): lax.scan(step_block, carried, (key_stack, value_stack, jnp.arange(block_c...]
  transfers between devices with their start and end apart: 7 -> 4, of which waited for: 6 -> 3; matrix products, arithmetic and copies ran while one was open for 8% -> 3% of each run, Pallas kernels for 0% -> 25%
where the time goes in v1:
time: 264 us
  waiting for transfers between devices  115 us (44%)
  Pallas kernels  65.9 us (25%)
  matrix products  26.4 us (10%)
  blocking collectives  22.3 us (8%)
  between operations  13.3 us (5%)
  local copies, waits for them, and re-layouts  9.4 us (4%)
  starting transfers between devices  7.56 us (3%)
  other arithmetic  4.24 us (2%)
    pallas_call x1, Pallas kernels, attention(): pl.pallas_call(functools.partial(attention_kernel, n, n_tp, tok_dev, coef...  65.9 us
    reduce_scatter x1, waiting for transfers between devices, shards(): lax.psum_scatter(jnp.dot(hidden, down_weight[0], preferred_element_type=j...  65.9 us
    all_gather x1, waiting for transfers between devices, shards(): rows_in = lax.all_gather(row_block, 'tp', axis=0, tiled=True)  39.7 us
    all_to_all x1, blocking collectives, shards(): lax.all_to_all(dispatch, 'sp', split_axis=0, concat_axis=0, tiled=True)  22.3 us
    dot_general x1, matrix products, shards(): jnp.dot(hidden, down_weight[0], preferred_element_type=jnp.float32)  13.2 us
    all_to_all x1, waiting for transfers between devices, shards(): lax.all_to_all(returned, 'sp', split_axis=0, concat_axis=0, tiled=True)  8.45 us
    dot_general x1, matrix products, shards(): jnp.dot(rows_in, gate_weight[0], preferred_element_type=jnp.float32)  7.87 us
    all_to_all x1, starting transfers between devices, shards(): lax.all_to_all(returned, 'sp', split_axis=0, concat_axis=0, tiled=True)  7.3 us
  transfers between devices with their start and end apart: 4, of which 3 were waited for; matrix products, arithmetic and copies ran while one was open for 3% of the time, Pallas kernels for 25%

profile of v1, /device:TPU:2, one launch (start us, length us, event | category | flops | bytes accessed | tf_op | source)
XLA Modules:
  0.0 263.9 jit_solution(14911835241133593964)
XLA Ops:
  6.5 0.7 all-gather.3.cloned.1.call-update
  7.3 0.7 multiply_bitcast_fusion
  8.0 0.6 broadcast_in_dim.4.bias_ref
  8.6 0.8 copy.16
  9.6 0.2 select_reduce_fusion
  9.8 1.1 fusion.15
  10.9 0.8 pad_maximum_fusion.1.q_ref
  11.7 1.1 fusion.13
  12.8 1.1 fusion.14
  13.8 0.1 maximum_bitcast_fusion
  14.0 0.8 pad_maximum_fusion.kv_ref
  14.8 65.9 %attention.1 = bf16[32,2048]{1,0:T(8,128)(2,1)} custom-call(bf16[512,128]{1,0:T(8,128)(2,1)} %pad_maximum_fusion.1.q_ref, bf16[2,512,128]{2,1,0:T(8,128)(2,1)} %pad_maximum_fusion.kv_ref, f32[2,1,512]{2,1,0:T(1,128)} %broadcast_in_dim.4.bias_ref), custom_call_target="tpu_custom_call" | custom-call | flops 18253611008 | bytes 4194304 | tf_op jit(solution)/shard_map/attention/pallas_call | solution.py:272
  80.7 5.1 %multiply_reduce_fusion.1 = (f32[32]{0:T(128)S(1)}, f32[32,2048]{1,0:T(8,128)S(1)}) fusion(bf16[32,2048]{1,0:T(8,128)(2,1)} %attention.1, bf16[2048,2048]{1,0:T(8,128)(2,1)} %all-gather.3.cloned.1.call-done, bf16[32,2048]{1,0:T(8,128)(2,1)S(1)} %copy-done.1), kind=kOutput, calls=%fused_computation.16 | convolution fusion | flops 268828640 | bytes 8913024 | tf_op jit(solution)/shard_map/dot_general | solution.py:324
  86.0 0.1 broadcast_in_dim.5
  86.3 0.2 convolution_convert_fusion.1
  86.5 0.1 reshape.71
  86.6 22.3 %all_to_all.10 = bf16[16,6,2048]{2,1,0:T(8,128)(2,1)S(1)} all-to-all(bf16[16,6,2048]{2,1,0:T(8,128)(2,1)S(1)} %reshape.71), channel_id=1, replica_groups=mesh['sp'=16,'tp'=16] {'sp'}, dimensions={0} | all-to-all | bytes 786432 | tf_op jit(solution)/shard_map/all_to_all | solution.py:347
  108.9 0.9 reshape.72
  109.8 0.2 reduce-scatter.2.cloned.1.call-start
  110.1 39.7 %all-gather.5.cloned.1.call-done = bf16[1536,2048]{1,0:T(8,128)(2,1)} async-done(((bf16[96,2048]{1,0:T(8,128)(2,1)}), bf16[1536,2048]{1,0:T(8,128)(2,1)}) %all-gather.5.cloned.1.call-update) | async-done | bytes 6291472 | tf_op jit(solution)/shard_map/all_gather | solution.py:349
  149.7 7.9 %fusion.5 = f32[1536,448]{0,1:T(8,128)} fusion(bf16[1536,2048]{1,0:T(8,128)(2,1)} %all-gather.5.cloned.1.call-done, bf16[1,2048,448]{1,2,0:T(8,128)(2,1)} %param.19), kind=kOutput, calls=%fused_computation.10 | convolution fusion | flops 2818572288 | bytes 10878976 | tf_op jit(solution)/shard_map/dot_general | solution.py:350
  157.6 13.2 %convolution_convert_fusion = bf16[1536,2048]{1,0:T(8,128)(2,1)} fusion(bf16[1,448,2048]{2,1,0:T(8,128)(2,1)S(1)} %copy-done, bf16[1536,2048]{1,0:T(8,128)(2,1)} %all-gather.5.cloned.1.call-done, f32[1536,448]{0,1:T(8,128)} %fusion.5, bf16[1,2048,448]{1,2,0:T(8,128)(2,1)} %param.20), kind=kOutput, calls=%fused_computation.1 | convolution fusion | flops 5644419072 | bytes 19005440 | tf_op jit(solution)/shard_map/dot_general | solution.py:354
  170.8 65.9 %reduce-scatter.2.cloned.1.call-done = bf16[96,2048]{1,0:T(8,128)(2,1)} async-done(((bf16[1536,2048]{1,0:T(8,128)(2,1)}), bf16[96,2048]{1,0:T(8,128)(2,1)}) %reduce-scatter.2.cloned.1.call-update) | async-done | bytes 393232 | tf_op jit(solution)/shard_map/reduce_scatter | solution.py:353
  236.7 1.9 reshape.73
  238.6 7.3 %all-to-all-start.1 = ((bf16[16,6,2048]{2,1,0:T(8,128)(2,1)}), bf16[16,6,2048]{2,1,0:T(8,128)(2,1)S(1)}, u32[]{:S(2)}, u32[]{:S(2)}) async-start(bf16[16,6,2048]{2,1,0:T(8,128)(2,1)} %reshape.73), calls=%async_computation.2 | async-start | bytes 1048576 | tf_op jit(solution)/shard_map/all_to_all | solution.py:360
  246.0 0.1 mul.81
  246.2 8.5 %all-to-all-done.1 = bf16[16,6,2048]{2,1,0:T(8,128)(2,1)S(1)} async-done(((bf16[16,6,2048]{2,1,0:T(8,128)(2,1)}), bf16[16,6,2048]{2,1,0:T(8,128)(2,1)S(1)}, u32[]{:S(2)}, u32[]{:S(2)}) %all-to-all-start.1) | async-done | bytes 393248 | tf_op jit(solution)/shard_map/all_to_all | solution.py:360
  254.7 0.1 reshape.74
  254.8 0.7 gather_fusion
  255.6 0.3 reshape.75
  255.9 0.7 multiply_reduce_fusion
  256.6 0.7 add_convert_fusion
  (27 shorter events, 0.8 us)
Async XLA Ops:
  6.5 151.1 %copy-start = (bf16[1,448,2048]{2,1,0:T(8,128)(2,1)S(1)}, bf16[1,448,2048]{2,1,0:T(8,128)(2,1)}, u32[]{:S(2)}) copy-start(bf16[1,448,2048]{2,1,0:T(8,128)(2,1)} %param.21) | copy-start | bytes 5505028
  6.5 74.2 %all-gather.3.cloned.1.call-start = ((), (), s32[]{:S(2)}) async-start(), calls=%async_computation.3 | async-start | bytes 8912896 | tf_op jit(solution)/shard_map/all_gather | solution.py:326
  7.3 142.5 %all-gather.5.cloned.1.call-start = ((), (), s32[]{:S(2)}) async-start(), calls=%async_computation.4 | async-start | bytes 6684672 | tf_op jit(solution)/shard_map/all_gather | solution.py:349
  14.8 66.0 %copy-start.1 = (bf16[32,2048]{1,0:T(8,128)(2,1)S(1)}, bf16[32,2048]{1,0:T(8,128)(2,1)}, u32[]{:S(2)}) copy-start(bf16[32,2048]{1,0:T(8,128)(2,1)} %param.12) | copy-start | bytes 393220
  80.7 5.2 %copy-start.2 = (f32[2048]{0:T(1024)S(1)}, f32[2048]{0:T(1024)}, u32[]{:S(2)}) copy-start(f32[2048]{0:T(1024)} %param.18) | copy-start | bytes 24580
  109.8 126.9 %reduce-scatter.2.cloned.1.call-start = ((), (), s32[]{:S(2)}) async-start(), calls=%async_computation.5 | async-start | bytes 6684672 | tf_op jit(solution)/shard_map/reduce_scatter | solution.py:353
  170.8 75.1 %copy-start.3 = (s32[32,2]{0,1:T(2,128)S(1)}, s32[32,2]{0,1:T(2,128)}, u32[]{:S(2)}) copy-start(s32[32,2]{0,1:T(2,128)} %param.22) | copy-start | bytes 772
  170.8 75.3 %copy-start.4 = (f32[32,2]{0,1:T(2,128)S(1)}, f32[32,2]{0,1:T(2,128)}, u32[]{:S(2)}) copy-start(f32[32,2]{0,1:T(2,128)} %param.23) | copy-start | bytes 772
  238.6 16.1 %all-to-all-start.1 = ((bf16[16,6,2048]{2,1,0:T(8,128)(2,1)}), bf16[16,6,2048]{2,1,0:T(8,128)(2,1)S(1)}, u32[]{:S(2)}, u32[]{:S(2)}) async-start(bf16[16,6,2048]{2,1,0:T(8,128)(2,1)} %reshape.73), calls=%async_computation.2 | async-start | bytes 1048576 | tf_op jit(solution)/shard_map/all_to_all | solution.py:360
Sparse Core Ops, SparseCore 0:
  9.2 58.7 all-gather.2
  109.9 39.7 all-gather.4
  171.0 65.6 reduce-scatter.1

commit v2 on v1

--- a/solution.py
+++ b/solution.py
@@ -302,6 +302,231 @@
         name="attention",
     )(q_swapped, kv, bias)
 
+def experts_kernel(
+    nz,
+    x_ref,
+    gate_hbm,
+    up_hbm,
+    down_hbm,
+    out_ref,
+    xbuf,
+    gate,
+    up,
+    down,
+    pown,
+    psend,
+    precv,
+    rsend,
+    rrecv,
+    w_sem,
+    x_sem,
+    ag_send,
+    ag_recv,
+    d_send,
+    d_recv,
+    p_send,
+    p_recv,
+    r_send,
+    r_recv,
+):
+    spi = lax.axis_index("sp")
+    tpi = lax.axis_index("tp")
+    z = lax.div(tpi, 2)
+    core = lax.rem(tpi, 2)
+    sign = 1 - 2 * core
+    nxt = (spi, lax.rem(z + sign + nz, nz) * 2 + core)
+    prv = (spi, lax.rem(z - sign + nz, nz) * 2 + core)
+    partner = (spi, z * 2 + 1 - core)
+    rows, model = x_ref.shape
+    subs = 2
+    half = rows // subs
+
+    def mine(k):
+        return lax.rem(z - sign * (1 + k) + 2 * nz, nz)
+
+    def theirs(k):
+        return lax.rem(z + sign * (1 + k) + 2 * nz, nz)
+
+    def part(s):
+        return pl.ds(s * half, half)
+
+    loads = [
+        pltpu.make_async_copy(a, b, w_sem.at[i])
+        for i, (a, b) in enumerate(((gate_hbm, gate), (up_hbm, up), (down_hbm, down)))
+    ]
+    for load in loads:
+        load.start()
+    own = pltpu.make_async_copy(x_ref, xbuf.at[core, z], x_sem)
+    own.start()
+
+    barrier = pltpu.get_barrier_semaphore()
+    for peer in (nxt, prv, partner):
+        pl.semaphore_signal(barrier, inc=1, device_id=peer, device_id_type=MESH)
+    pl.semaphore_wait(barrier, 3)
+    own.wait()
+
+    def ring(k, s):
+        return pltpu.make_async_remote_copy(
+            src_ref=xbuf.at[core, mine(k), part(s)],
+            dst_ref=xbuf.at[core, mine(k), part(s)],
+            send_sem=ag_send.at[k, s],
+            recv_sem=ag_recv.at[lax.rem(k + 1, nz), s],
+            device_id=nxt,
+            device_id_type=MESH,
+        )
+
+    def share(k):
+        return pltpu.make_async_remote_copy(
+            src_ref=xbuf.at[core, mine(k)],
+            dst_ref=xbuf.at[core, mine(k)],
+            send_sem=d_send.at[k],
+            recv_sem=d_recv.at[k],
+            device_id=partner,
+            device_id_type=MESH,
+        )
+
+    def give(k, s):
+        return pltpu.make_async_remote_copy(
+            src_ref=psend.at[k, part(s)],
+            dst_ref=precv.at[k, part(s)],
+            send_sem=p_send.at[k, s],
+            recv_sem=p_recv.at[k, s],
+            device_id=partner,
+            device_id_type=MESH,
+        )
+
+    def reduce(k, s):
+        return pltpu.make_async_remote_copy(
+            src_ref=rsend.at[k, part(s)],
+            dst_ref=rrecv.at[k, part(s)],
+            send_sem=r_send.at[k, s],
+            recv_sem=r_recv.at[k, s],
+            device_id=nxt,
+            device_id_type=MESH,
+        )
+
+    for s in range(subs):
+        ring(nz - 1, s).start()
+    share(nz - 1).start()
+    for load in loads:
+        load.wait()
+
+    tile = min(512, model)
+
+    def step(k, c):
+        @pl.when(k < nz - 1)
+        def _():
+            for s in range(subs):
+                pltpu.make_async_copy(
+                    xbuf.at[core, 0, part(s)], xbuf.at[core, mine(k), part(s)], ag_recv.at[k, s]
+                ).wait()
+
+                @pl.when(k < nz - 2)
+                def _():
+                    ring(k, s).start()
+
+            share(k).start()
+
+        pltpu.make_async_copy(
+            xbuf.at[1 - core, 0], xbuf.at[1 - core, theirs(k)], d_recv.at[k]
+        ).wait()
+
+        x = jnp.concatenate([xbuf[1 - core, theirs(k)], xbuf[core, mine(k)]], axis=0)
+        g = jnp.dot(x, gate[...], preferred_element_type=jnp.float32)
+        u = jnp.dot(x, up[...], preferred_element_type=jnp.float32)
+        hidden = (g / (1.0 + jnp.exp(-g)) * u).astype(jnp.bfloat16)
+        for n in range(model // tile):
+            cols = slice(n * tile, (n + 1) * tile)
+            p = jnp.dot(hidden, down[:, cols], preferred_element_type=jnp.float32)
+            psend[k, :, cols] = p[:rows].astype(jnp.bfloat16)
+            pown[:, cols] = p[rows:]
+        for s in range(subs):
+            give(k, s).start()
+        for s in range(subs):
+            give(k, s).wait_recv()
+            total = pown[part(s), :] + precv[k, part(s), :].astype(jnp.float32)
+
+            @pl.when(k > 0)
+            def _():
+                kk = jnp.maximum(k - 1, 0)
+                reduce(kk, s).wait_recv()
+                pown[part(s), :] = total + rrecv[kk, part(s), :].astype(jnp.float32)
+
+            @pl.when(k == 0)
+            def _():
+                pown[part(s), :] = total
+
+            @pl.when(k < nz - 1)
+            def _():
+                rsend[k, part(s), :] = pown[part(s), :].astype(jnp.bfloat16)
+                reduce(k, s).start()
+
+        return c
+
+    lax.fori_loop(0, nz, step, 0)
+    out_ref[...] = pown[...].astype(jnp.bfloat16)
+
+    def drain(k, c):
+        for s in range(subs):
+            give(k, s).wait_send()
+
+            @pl.when(k != nz - 2)
+            def _():
+                ring(k, s).wait_send()
+
+            @pl.when(k < nz - 1)
+            def _():
+                reduce(k, s).wait_send()
+
+        share(k).wait_send()
+        return c
+
+    lax.fori_loop(0, nz, drain, 0)
+
+
+def experts(x, gate_weight, up_weight, down_weight):
+    nz = lax.axis_size("tp") // 2
+    rows, model = x.shape
+    inner = gate_weight.shape[1]
+    vmem = pl.BlockSpec(memory_space=pltpu.VMEM)
+    hbm = pl.BlockSpec(memory_space=pl.ANY)
+    bf16 = jnp.bfloat16
+    dma = pltpu.SemaphoreType.DMA
+    return pl.pallas_call(
+        functools.partial(experts_kernel, nz),
+        out_shape=jax.ShapeDtypeStruct((rows, model), bf16),
+        in_specs=[vmem, hbm, hbm, hbm],
+        out_specs=vmem,
+        scratch_shapes=[
+            pltpu.VMEM((2, nz, rows, model), bf16),
+            pltpu.VMEM((model, inner), bf16),
+            pltpu.VMEM((model, inner), bf16),
+            pltpu.VMEM((inner, model), bf16),
+            pltpu.VMEM((rows, model), jnp.float32),
+            pltpu.VMEM((nz, rows, model), bf16),
+            pltpu.VMEM((nz, rows, model), bf16),
+            pltpu.VMEM((nz - 1, rows, model), bf16),
+            pltpu.VMEM((nz - 1, rows, model), bf16),
+            dma((3,)),
+            dma,
+            dma((nz, 2)),
+            dma((nz, 2)),
+            dma((nz,)),
+            dma((nz,)),
+            dma((nz, 2)),
+            dma((nz, 2)),
+            dma((nz - 1, 2)),
+            dma((nz - 1, 2)),
+        ],
+        compiler_params=pltpu.CompilerParams(
+            collective_id=1, has_side_effects=True, vmem_limit_bytes=60 << 20
+        ),
+        cost_estimate=pl.CostEstimate(
+            flops=2 * nz * rows * 2 * model * inner * 3, bytes_accessed=8 << 20, transcendentals=0
+        ),
+        name="experts",
+    )(x, gate_weight, up_weight, down_weight)
+
 
 def shards(
     tokens,
@@ -346,16 +571,7 @@
     dispatch = dispatch.reshape(n_experts, capacity, model_width)
     arrived = lax.all_to_all(dispatch, "sp", split_axis=0, concat_axis=0, tiled=True)
     row_block = arrived.reshape(-1, model_width)
-    rows_in = lax.all_gather(row_block, "tp", axis=0, tiled=True)
-    gate_value = jnp.dot(rows_in, gate_weight[0], preferred_element_type=jnp.float32)
-    up_value = jnp.dot(rows_in, up_weight[0], preferred_element_type=jnp.float32)
-    hidden = (jax.nn.silu(gate_value) * up_value).astype(jnp.bfloat16)
-    summed = lax.psum_scatter(
-        jnp.dot(hidden, down_weight[0], preferred_element_type=jnp.float32).astype(jnp.bfloat16),
-        "tp",
-        scatter_dimension=0,
-        tiled=True,
-    )
+    summed = experts(row_block, gate_weight[0], up_weight[0], down_weight[0])
     returned = summed.reshape(arrived.shape)
     back = lax.all_to_all(returned, "sp", split_axis=0, concat_axis=0, tiled=True)
     flat_back = back.reshape(n_experts * capacity, model_width)

time: 264 us -> 209 us (0.79)
  waiting for transfers between devices: 115 us -> 15.5 us
  Pallas kernels: 65.9 us -> 136 us
  blocking collectives: 22.3 us -> 0 us
  matrix products: 26.4 us -> 5.36 us
  starting transfers between devices: 7.56 us -> 16.9 us
  local copies, waits for them, and re-layouts: 9.4 us -> 15.5 us
    pallas_call x0 -> x1, Pallas kernels: none -> 70.1 us  [experts(): pl.pallas_call(functools.partial(experts_kernel, nz), out_shape=jax.Shape...]
    reduce_scatter x1 -> x0, waiting for transfers between devices: 65.9 us -> none  [shards(): lax.psum_scatter(jnp.dot(hidden, down_weight[0], preferred_element_type=j...]
    all_gather x1 -> x0, waiting for transfers between devices: 39.7 us -> none  [shards(): rows_in = lax.all_gather(row_block, 'tp', axis=0, tiled=True)]
    all_to_all x1 -> x0, blocking collectives: 22.3 us -> none  [shards(): lax.all_to_all(dispatch, 'sp', split_axis=0, concat_axis=0, tiled=True)]
    dot_general x2 -> x0, matrix products: 21.1 us -> none  [the longest x1 13.2 us: shards(): jnp.dot(hidden, down_weight[0], preferred_element_type=jnp.float32)]
    all_to_all x0 -> x1, starting transfers between devices: none -> 12.1 us  [shards(): lax.all_to_all(dispatch, 'sp', split_axis=0, concat_axis=0, tiled=True)]
    unnamed x12 -> x16, local copies, waits for them, and re-layouts: 0.87 us -> 7.13 us
    all_to_all x0 -> x1, waiting for transfers between devices: none -> 4.2 us  [shards(): lax.all_to_all(dispatch, 'sp', split_axis=0, concat_axis=0, tiled=True)]
  transfers between devices with their start and end apart: 4 -> 3, of which waited for: 3 -> 2; matrix products, arithmetic and copies ran while one was open for 3% -> 6% of each run, Pallas kernels for 25% -> 32%
where the time goes in v2:
time: 209 us; the launch traced here: 207 us
  Pallas kernels  136 us (65%)
  starting transfers between devices  16.9 us (8%)
  local copies, waits for them, and re-layouts  15.5 us (7%)
  waiting for transfers between devices  15.5 us (7%)
  between operations  13.6 us (7%)
  matrix products  5.36 us (3%)
  other arithmetic  4.23 us (2%)
    pallas_call x1, Pallas kernels, experts(): pl.pallas_call(functools.partial(experts_kernel, nz), out_shape=jax.Shape...  70.1 us
    pallas_call x1, Pallas kernels, attention(): pl.pallas_call(functools.partial(attention_kernel, n, n_tp, tok_dev, coef...  65.9 us
    all_to_all x1, starting transfers between devices, shards(): lax.all_to_all(dispatch, 'sp', split_axis=0, concat_axis=0, tiled=True)  12.1 us
    all_to_all x1, waiting for transfers between devices, shards(): lax.all_to_all(returned, 'sp', split_axis=0, concat_axis=0, tiled=True)  10.6 us
    unnamed x16, local copies, waits for them, and re-layouts  7.13 us
    dot_general x1, matrix products, shards(): jnp.dot(token_rows, lax.all_gather(out_weight, 'tp', axis=0, tiled=True),...  5.12 us
    all_to_all x1, starting transfers between devices, shards(): lax.all_to_all(returned, 'sp', split_axis=0, concat_axis=0, tiled=True)  4.82 us
    all_to_all x1, waiting for transfers between devices, shards(): lax.all_to_all(dispatch, 'sp', split_axis=0, concat_axis=0, tiled=True)  4.2 us
  transfers between devices with their start and end apart: 3, of which 2 were waited for; matrix products, arithmetic and copies ran while one was open for 6% of the time, Pallas kernels for 32%

profile of v2, /device:TPU:2, one launch (start us, length us, event | category | flops | bytes accessed | tf_op | source)
XLA Modules:
  0.0 207.1 jit_solution(11684700883796539239)
XLA Ops:
  6.5 0.7 all-gather.2.cloned.1.call-update
  7.3 0.7 multiply_bitcast_fusion
  7.9 0.6 broadcast_in_dim.4.bias_ref
  8.5 0.8 copy.18
  9.3 0.1 reshape.69
  9.6 0.2 select_reduce_fusion
  9.8 1.1 fusion.7
  10.9 0.8 pad_maximum_fusion.1.q_ref
  11.6 1.1 fusion.5
  12.7 0.1 fusion.6
  12.8 0.1 maximum_bitcast_fusion
  13.0 0.8 pad_maximum_fusion.kv_ref
  13.8 65.9 %attention.1 = bf16[32,2048]{1,0:T(8,128)(2,1)} custom-call(bf16[512,128]{1,0:T(8,128)(2,1)} %pad_maximum_fusion.1.q_ref, bf16[2,512,128]{2,1,0:T(8,128)(2,1)} %pad_maximum_fusion.kv_ref, f32[2,1,512]{2,1,0:T(1,128)} %broadcast_in_dim.4.bias_ref), custom_call_target="tpu_custom_call" | custom-call | flops 18253611008 | bytes 4194304 | tf_op jit(solution)/shard_map/attention/pallas_call | solution.py:272
  79.7 5.1 %multiply_reduce_fusion.1 = (f32[32]{0:T(128)S(1)}, f32[32,2048]{1,0:T(8,128)S(1)}) fusion(bf16[32,2048]{1,0:T(8,128)(2,1)} %attention.1, bf16[2048,2048]{1,0:T(8,128)(2,1)} %all-gather.2.cloned.1.call-done, bf16[32,2048]{1,0:T(8,128)(2,1)S(1)} %copy-done.2), kind=kOutput, calls=%fused_computation.9 | convolution fusion | flops 268828640 | bytes 8913024 | tf_op jit(solution)/shard_map/dot_general | solution.py:549
  84.9 0.1 broadcast_in_dim.5
  85.2 0.2 convolution_convert_fusion
  85.5 0.9 reshape.71
  86.4 12.1 %all-to-all-start = ((bf16[16,6,2048]{2,1,0:T(8,128)(2,1)}), bf16[16,6,2048]{2,1,0:T(8,128)(2,1)S(1)}, u32[]{:S(2)}, u32[]{:S(2)}) async-start(bf16[16,6,2048]{2,1,0:T(8,128)(2,1)} %reshape.71), calls=%async_computation | async-start | bytes 1048576 | tf_op jit(solution)/shard_map/all_to_all | solution.py:572
  98.5 2.4 %copy.19 = bf16[1,2048,448]{2,1,0:T(8,128)(2,1)} copy(bf16[1,2048,448]{1,2,0:T(8,128)(2,1)S(1)} %copy-done) | data formatting | bytes 3670016 | tf_op args[7]
  100.9 3.8 %copy.20 = bf16[1,2048,448]{2,1,0:T(8,128)(2,1)} copy(bf16[1,2048,448]{1,2,0:T(8,128)(2,1)} %param.20) | data formatting | bytes 3670016 | tf_op args[8]
  104.8 4.2 %all-to-all-done = bf16[16,6,2048]{2,1,0:T(8,128)(2,1)S(1)} async-done(((bf16[16,6,2048]{2,1,0:T(8,128)(2,1)}), bf16[16,6,2048]{2,1,0:T(8,128)(2,1)S(1)}, u32[]{:S(2)}, u32[]{:S(2)}) %all-to-all-start) | async-done | bytes 393248 | tf_op jit(solution)/shard_map/all_to_all | solution.py:572
  108.9 0.9 reshape.72.x_ref
  109.9 70.1 %experts.1 = bf16[96,2048]{1,0:T(8,128)(2,1)} custom-call(bf16[96,2048]{1,0:T(8,128)(2,1)} %reshape.72.x_ref, bf16[2048,448]{1,0:T(8,128)(2,1)} %bitcast.18, bf16[2048,448]{1,0:T(8,128)(2,1)} %bitcast.19, bf16[448,2048]{1,0:T(8,128)(2,1)} %bitcast.20), custom_call_target="tpu_custom_call" | custom-call | flops 8455716864 | bytes 8388608 | tf_op jit(solution)/shard_map/experts/pallas_call | solution.py:495
  179.9 1.9 reshape.73
  181.9 4.8 %all-to-all-start.1 = ((bf16[16,6,2048]{2,1,0:T(8,128)(2,1)}), bf16[16,6,2048]{2,1,0:T(8,128)(2,1)S(1)}, u32[]{:S(2)}, u32[]{:S(2)}) async-start(bf16[16,6,2048]{2,1,0:T(8,128)(2,1)} %reshape.73), calls=%async_computation.1 | async-start | bytes 1048576 | tf_op jit(solution)/shard_map/all_to_all | solution.py:576
  186.8 0.1 mul.72
  187.0 10.6 %all-to-all-done.1 = bf16[16,6,2048]{2,1,0:T(8,128)(2,1)S(1)} async-done(((bf16[16,6,2048]{2,1,0:T(8,128)(2,1)}), bf16[16,6,2048]{2,1,0:T(8,128)(2,1)S(1)}, u32[]{:S(2)}, u32[]{:S(2)}) %all-to-all-start.1) | async-done | bytes 393248 | tf_op jit(solution)/shard_map/all_to_all | solution.py:576
  197.6 0.1 reshape.74
  197.7 0.7 gather_fusion
  198.5 0.3 reshape.75
  198.8 0.7 multiply_reduce_fusion
  199.6 0.7 add_convert_fusion
  (25 shorter events, 0.6 us)
Async XLA Ops:
  6.5 6.2 %copy-start.1 = (bf16[512,128]{1,0:T(8,128)(2,1)S(1)}, bf16[512,128]{1,0:T(8,128)(2,1)}, u32[]{:S(2)}) copy-start(bf16[512,128]{1,0:T(8,128)(2,1)} %param.14) | copy-start | bytes 393220
  6.5 73.1 %all-gather.2.cloned.1.call-start = ((), (), s32[]{:S(2)}) async-start(), calls=%async_computation.2 | async-start | bytes 8912896 | tf_op jit(solution)/shard_map/all_gather | solution.py:551
  13.7 65.9 %copy-start.2 = (bf16[32,2048]{1,0:T(8,128)(2,1)S(1)}, bf16[32,2048]{1,0:T(8,128)(2,1)}, u32[]{:S(2)}) copy-start(bf16[32,2048]{1,0:T(8,128)(2,1)} %param.12) | copy-start | bytes 393220
  79.6 5.2 %copy-start.3 = (f32[2048]{0:T(1024)S(1)}, f32[2048]{0:T(1024)}, u32[]{:S(2)}) copy-start(f32[2048]{0:T(1024)} %param.18) | copy-start | bytes 24580
  84.8 13.7 %copy-start = (bf16[1,2048,448]{1,2,0:T(8,128)(2,1)S(1)}, bf16[1,2048,448]{1,2,0:T(8,128)(2,1)}, u32[]{:S(2)}) copy-start(bf16[1,2048,448]{1,2,0:T(8,128)(2,1)} %param.19) | copy-start | bytes 5505028
  86.4 22.5 %all-to-all-start = ((bf16[16,6,2048]{2,1,0:T(8,128)(2,1)}), bf16[16,6,2048]{2,1,0:T(8,128)(2,1)S(1)}, u32[]{:S(2)}, u32[]{:S(2)}) async-start(bf16[16,6,2048]{2,1,0:T(8,128)(2,1)} %reshape.71), calls=%async_computation | async-start | bytes 1048576 | tf_op jit(solution)/shard_map/all_to_all | solution.py:572
  109.9 76.8 %copy-start.4 = (s32[32,2]{0,1:T(2,128)S(1)}, s32[32,2]{0,1:T(2,128)}, u32[]{:S(2)}) copy-start(s32[32,2]{0,1:T(2,128)} %param.22) | copy-start | bytes 772
  109.9 77.0 %copy-start.5 = (f32[32,2]{0,1:T(2,128)S(1)}, f32[32,2]{0,1:T(2,128)}, u32[]{:S(2)}) copy-start(f32[32,2]{0,1:T(2,128)} %param.23) | copy-start | bytes 772
  181.9 15.8 %all-to-all-start.1 = ((bf16[16,6,2048]{2,1,0:T(8,128)(2,1)}), bf16[16,6,2048]{2,1,0:T(8,128)(2,1)S(1)}, u32[]{:S(2)}, u32[]{:S(2)}) async-start(bf16[16,6,2048]{2,1,0:T(8,128)(2,1)} %reshape.73), calls=%async_computation.1 | async-start | bytes 1048576 | tf_op jit(solution)/shard_map/all_to_all | solution.py:576
Sparse Core Ops, SparseCore 0:
  9.2 58.7 all-gather.1

commit v3 on v2

v3 whole, which is shorter than its diff:
```python
import functools
import math

import jax
import jax.numpy as jnp
from jax import lax
from jax.experimental import pallas as pl
from jax.experimental.pallas import tpu as pltpu
from jax.sharding import PartitionSpec as P

NEG_LARGE = -1e30
MESH = pl.DeviceIdType.MESH
SLOTS = 8


def attention_kernel(
    n,
    n_tp,
    coef,
    q_ref,
    k_ref,
    v_ref,
    gate_ref,
    w_ref,
    tok_ref,
    gain_ref,
    stream_ref,
    normed_ref,
    qraw,
    qbuf,
    kvsend,
    bsend,
    kvbuf,
    bbuf,
    peak,
    total,
    acc,
    obuf,
    rbuf,
    wbuf,
    proj,
    kv_send,
    kv_recv,
    b_send,
    b_recv,
    q_send,
    q_recv,
    o_send,
    o_recv,
    w_send,
    w_recv,
    d_send,
    d_recv,
    own_sem,
):
    me = lax.axis_index("sp")
    mt = lax.axis_index("tp")
    nz = n_tp // 2
    z = lax.div(mt, 2)
    core = lax.rem(mt, 2)
    sign = 1 - 2 * core
    nxt = (me, lax.rem(z + sign + nz, nz) * 2 + core)
    partner = (me, z * 2 + 1 - core)
    mirror = n - 1 - me
    head = lax.div(me, n // 2)
    pair = jnp.minimum(me, mirror)
    last = jnp.maximum(me, mirror)
    own_slot = head
    rows, width = q_ref.shape
    half = width // 2
    tok_dev, model = tok_ref.shape

    barrier = pltpu.get_barrier_semaphore()

    def greet_plane(k, c):
        pl.semaphore_signal(
            barrier, inc=1, device_id=(lax.rem(me + k, n), mt), device_id_type=MESH
        )
        return c

    def greet_heads(k, c):
        t = lax.rem(mt + k, n_tp)
        pl.semaphore_signal(barrier, inc=1, device_id=(me, t), device_id_type=MESH)
        pl.semaphore_signal(barrier, inc=1, device_id=(mirror, t), device_id_type=MESH)
        return c

    lax.fori_loop(1, n, greet_plane, 0)
    lax.fori_loop(1, n_tp, greet_heads, 0)

    own_w = pltpu.make_async_copy(w_ref, wbuf.at[mt], own_sem.at[0])
    own_w.start()
    lane = lax.broadcasted_iota(jnp.int32, (rows, width), 1)
    low = lane < half
    rolled_k = pltpu.roll(k_ref[...].astype(jnp.float32), half, 1)
    values = v_ref[...].astype(jnp.float32)
    kvsend[0] = jnp.where(low, values, rolled_k).astype(jnp.bfloat16)
    kvsend[1] = jnp.where(low, rolled_k, values).astype(jnp.bfloat16)
    bias_rows = gate_ref[...] * (-math.log2(math.e))
    bsend[0] = bias_rows[0:1]
    bsend[1] = bias_rows[1:2]
    mine = low == (head == 1)

    def prepare(raw):
        rolled = pltpu.roll(raw.astype(jnp.float32), half, 1)
        return jnp.where(mine, rolled, 0.0).astype(jnp.bfloat16)

    qbuf[own_slot] = prepare(q_ref[...])
    peak[...] = jnp.full(peak.shape, NEG_LARGE, jnp.float32)
    total[...] = jnp.zeros(total.shape, jnp.float32)
    acc[...] = jnp.zeros(acc.shape, jnp.float32)

    pl.semaphore_wait(barrier, (n - 1) + 2 * (n_tp - 1))

    q_copy = pltpu.make_async_remote_copy(
        src_ref=q_ref,
        dst_ref=qraw,
        send_sem=q_send,
        recv_sem=q_recv,
        device_id=(mirror, mt),
        device_id_type=MESH,
    )
    q_copy.start()

    w_half = w_ref.shape[0] // 2

    def w_mine(k):
        return lax.rem(z - sign * (1 + k) + 2 * nz, nz) * 2 + core

    def w_theirs(k):
        return lax.rem(z + sign * (1 + k) + 2 * nz, nz) * 2 + 1 - core

    def w_ring(k, s, src):
        return pltpu.make_async_remote_copy(
            src_ref=src.at[pl.ds(s * w_half, w_half)],
            dst_ref=wbuf.at[w_mine(k), pl.ds(s * w_half, w_half)],
            send_sem=w_send.at[k, s],
            recv_sem=w_recv.at[lax.rem(k + 1, nz), s],
            device_id=nxt,
            device_id_type=MESH,
        )

    def w_share(k, s, src):
        return pltpu.make_async_remote_copy(
            src_ref=src.at[pl.ds(s * w_half, w_half)],
            dst_ref=wbuf.at[w_mine(k), pl.ds(s * w_half, w_half)],
            send_sem=d_send.at[k, s],
            recv_sem=d_recv.at[k, s],
            device_id=partner,
            device_id_type=MESH,
        )

    for s in range(2):
        w_ring(nz - 1, s, w_ref).start()

    def kv_copy(r):
        hr = lax.div(r, n // 2)
        return (
            pltpu.make_async_remote_copy(
                src_ref=kvsend.at[hr],
                dst_ref=kvbuf.at[me],
                send_sem=kv_send.at[r],
                recv_sem=kv_recv.at[me],
                device_id=(r, mt),
                device_id_type=MESH,
            ),
            pltpu.make_async_remote_copy(
                src_ref=bsend.at[hr],
                dst_ref=bbuf.at[me],
                send_sem=b_send.at[r],
                recv_sem=b_recv.at[me],
                device_id=(r, mt),
                device_id_type=MESH,
            ),
        )

    def send_body(k, c):
        r = lax.rem(me + k, n)

        @pl.when(me <= jnp.maximum(r, n - 1 - r))
        def _():
            ck, cb = kv_copy(r)
            cb.start()
            ck.start()

        return c

    lax.fori_loop(1, n, send_body, 0)
    for s in range(2):
        w_share(nz - 1, s, w_ref).start()

    sub = min(256, rows)

    def tile(slot, kv_at, bias_at, diagonal):
        for i in range(rows // sub):
            kv = kv_at[...]
            rs = pl.ds(i * sub, sub)
            s = lax.dot_general(
                qbuf[slot, rs, :], kv, (((1,), (1,)), ((), ())), preferred_element_type=jnp.float32
            )
            s = s * coef + bias_at[...]
            if diagonal:
                qp = lax.broadcasted_iota(jnp.int32, s.shape, 0) + i * sub
                kp = lax.broadcasted_iota(jnp.int32, s.shape, 1)
                s = jnp.where(kp <= qp, s, NEG_LARGE)
            old = peak[slot, rs, :]
            new = jnp.maximum(old, jnp.max(s, axis=1, keepdims=True))
            e = jnp.exp2(s - new)
            alpha = jnp.exp2(old - new)
            total[slot, rs, :] = total[slot, rs, :] * alpha + jnp.sum(e, axis=1, keepdims=True)
            acc[slot, rs, :] = acc[slot, rs, :] * alpha + jnp.dot(
                e.astype(jnp.bfloat16), kv, preferred_element_type=jnp.float32
            )
            peak[slot, rs, :] = new

    tile(own_slot, kvsend.at[head], bsend.at[head], True)
    pltpu.make_async_copy(q_ref, qraw, q_recv).wait()
    qbuf[1 - own_slot] = prepare(qraw[...])

    @pl.when(me < last)
    def _():
        tile(1, kvsend.at[head], bsend.at[head], False)

    def w_event(i):
        k = lax.div(i, 2)
        s = lax.rem(i, 2)
        block = wbuf.at[w_mine(k)]
        pltpu.make_async_copy(
            w_ref.at[pl.ds(0, w_half)], block.at[pl.ds(s * w_half, w_half)], w_recv.at[k, s]
        ).wait()

        @pl.when(k < nz - 2)
        def _():
            w_ring(k, s, block).start()

        w_share(k, s, block).start()

    events = 2 * (nz - 1)
    early = min(nz - 1, (n - 1) // 2)

    def compute_body(k, c):
        j = lax.rem(me - k + n, n)

        @pl.when(jnp.logical_and(lax.rem(k, 2) == 0, lax.div(k, 2) <= early))
        def _():
            w_event(lax.div(k, 2) - 1)

        @pl.when(j <= last)
        def _():
            pltpu.make_async_copy(kvsend.at[0], kvbuf.at[j], kv_recv.at[j]).wait()
            pltpu.make_async_copy(bsend.at[0], bbuf.at[j], b_recv.at[j]).wait()

            def slot_body(slot, c):
                end = jnp.where(slot == 0, pair, last)

                @pl.when(j == end)
                def _():
                    tile(slot, kvbuf.at[j], bbuf.at[j], True)

                @pl.when(j < end)
                def _():
                    tile(slot, kvbuf.at[j], bbuf.at[j], False)

                return c

            lax.fori_loop(0, 2, slot_body, 0)

        return c

    lax.fori_loop(1, n, compute_body, 0)

    for slot in range(2):
        obuf[slot] = (acc[slot] / total[slot]).astype(jnp.bfloat16)

    def o_target(slot):
        return jnp.where(slot == 0, pair, last)

    def o_copy(slot, t):
        return pltpu.make_async_remote_copy(
            src_ref=obuf.at[slot, pl.ds(t * tok_dev, tok_dev)],
            dst_ref=rbuf.at[mt, head],
            send_sem=o_send.at[slot, t],
            recv_sem=o_recv,
            device_id=(o_target(slot), t),
            device_id_type=MESH,
        )

    def o_self(slot, t):
        return jnp.logical_and(o_target(slot) == me, t == mt)

    def o_body(k, c):
        slot = lax.rem(k, 2)
        t = lax.rem(mt + n_tp // 2 + lax.div(k, 2), n_tp)

        @pl.when(jnp.logical_not(o_self(slot, t)))
        def _():
            o_copy(slot, t).start()

        @pl.when(o_self(slot, t))
        def _():
            pltpu.make_async_copy(
                obuf.at[slot, pl.ds(t * tok_dev, tok_dev)], rbuf.at[mt, head], o_recv
            ).start()

        return c

    lax.fori_loop(0, 2 * n_tp, o_body, 0)

    def late_event(i, c):
        w_event(i)
        return c

    steps_before = min(5, nz - 1)
    lax.fori_loop(early, 2 * steps_before, late_event, 0)

    pltpu.make_async_copy(rbuf, rbuf, o_recv).wait()
    own_w.wait()
    for s in range(2):
        pltpu.make_async_copy(
            w_ref.at[pl.ds(0, w_half)], wbuf.at[mt, pl.ds(s * w_half, w_half)], d_recv.at[nz - 1, s]
        ).wait()
    low32 = lax.broadcasted_iota(jnp.int32, (tok_dev, width), 1) < half

    def product(t):
        piece = jnp.where(
            low32, rbuf[t, 0].astype(jnp.float32), rbuf[t, 1].astype(jnp.float32)
        ).astype(jnp.bfloat16)
        return jnp.dot(piece, wbuf[t], preferred_element_type=jnp.float32)

    proj[...] = product(mt)
    proj[...] += product(z * 2 + 1 - core)

    def project(k, c):
        @pl.when(k >= steps_before)
        def _():
            for s in range(2):
                w_event(2 * k + s)

        for s in range(2):
            pltpu.make_async_copy(
                w_ref.at[pl.ds(0, w_half)],
                wbuf.at[w_theirs(k), pl.ds(s * w_half, w_half)],
                d_recv.at[k, s],
            ).wait()
        proj[...] += product(w_mine(k))
        proj[...] += product(w_theirs(k))
        return c

    lax.fori_loop(0, nz - 1, project, 0)
    stream = (tok_ref[...].astype(jnp.float32) + proj[...]).astype(jnp.bfloat16)
    stream_ref[...] = stream
    wide = stream.astype(jnp.float32)
    inverse = lax.rsqrt(jnp.mean(wide * wide, axis=1, keepdims=True) + 1e-05)
    normed_ref[...] = (wide * inverse * gain_ref[...]).astype(jnp.bfloat16)

    q_copy.wait_send()

    def drain_body(k, c):
        r = lax.rem(me + k, n)

        @pl.when(me <= jnp.maximum(r, n - 1 - r))
        def _():
            ck, cb = kv_copy(r)
            cb.wait_send()
            ck.wait_send()

        return c

    lax.fori_loop(1, n, drain_body, 0)

    def o_drain(k, c):
        slot = lax.rem(k, 2)
        t = lax.div(k, 2)

        @pl.when(jnp.logical_not(o_self(slot, t)))
        def _():
            o_copy(slot, t).wait_send()

        return c

    lax.fori_loop(0, 2 * n_tp, o_drain, 0)

    def w_drain(k, c):
        for s in range(2):
            w_share(k, s, w_ref).wait_send()

            @pl.when(k != nz - 2)
            def _():
                w_ring(k, s, w_ref).wait_send()

        return c

    lax.fori_loop(0, nz, w_drain, 0)


def attention(query_vectors, key_vectors, value_vectors, cum_gate, out_weight, tokens, norm_gain):
    n = lax.axis_size("sp")
    n_tp = lax.axis_size("tp")
    nz = n_tp // 2
    rows, width = query_vectors.shape
    tok_dev, model = tokens.shape
    coef = (width // 2) ** (-0.5) * math.log2(math.e)
    vmem = pl.BlockSpec(memory_space=pltpu.VMEM)
    bf16, f32 = jnp.bfloat16, jnp.float32
    dma = pltpu.SemaphoreType.DMA
    result = jax.ShapeDtypeStruct((tok_dev, model), bf16)
    return pl.pallas_call(
        functools.partial(attention_kernel, n, n_tp, coef),
        out_shape=(result, result),
        in_specs=[vmem] * 7,
        out_specs=(vmem, vmem),
        scratch_shapes=[
            pltpu.VMEM((rows, width), bf16),
            pltpu.VMEM((2, rows, width), bf16),
            pltpu.VMEM((2, rows, width), bf16),
            pltpu.VMEM((2, 1, rows), f32),
            pltpu.VMEM((n, rows, width), bf16),
            pltpu.VMEM((n, 1, rows), f32),
            pltpu.VMEM((2, rows, 1), f32),
            pltpu.VMEM((2, rows, 1), f32),
            pltpu.VMEM((2, rows, width), f32),
            pltpu.VMEM((2, rows, width), bf16),
            pltpu.VMEM((n_tp, 2, tok_dev, width), bf16),
            pltpu.VMEM((n_tp, width, model), bf16),
            pltpu.VMEM((tok_dev, model), f32),
            dma((n,)),
            dma((n,)),
            dma((n,)),
            dma((n,)),
            dma,
            dma,
            dma((2, n_tp)),
            dma,
            dma((nz, 2)),
            dma((nz, 2)),
            dma((nz, 2)),
            dma((nz, 2)),
            dma((1,)),
        ],
        compiler_params=pltpu.CompilerParams(
            collective_id=0, has_side_effects=True, vmem_limit_bytes=48 << 20
        ),
        name="attention",
    )(
        query_vectors,
        key_vectors,
        value_vectors,
        cum_gate.T,
        out_weight,
        tokens,
        norm_gain[None, :],
    )


def experts_kernel(
    nz,
    n,
    capacity,
    normed_ref,
    stream_ref,
    place_ref,
    pick_ref,
    route_ref,
    gate_hbm,
    up_hbm,
    down_hbm,
    out_ref,
    packed,
    arrived,
    xbuf,
    gate,
    up,
    down,
    pown,
    psend,
    precv,
    rsend,
    rrecv,
    spread,
    back,
    w_sem,
    a_send,
    a_recv,
    b_send,
    b_recv,
    ag_send,
    ag_recv,
    d_send,
    d_recv,
    p_send,
    p_recv,
    r_send,
    r_recv,
):
    spi = lax.axis_index("sp")
    tpi = lax.axis_index("tp")
    z = lax.div(tpi, 2)
    core = lax.rem(tpi, 2)
    sign = 1 - 2 * core
    nxt = (spi, lax.rem(z + sign + nz, nz) * 2 + core)
    prv = (spi, lax.rem(z - sign + nz, nz) * 2 + core)
    partner = (spi, z * 2 + 1 - core)
    model = normed_ref.shape[1]
    rows = n * capacity
    padded = n * SLOTS
    subs = 2
    half = rows // subs
    bf16, f32 = jnp.bfloat16, jnp.float32

    loads = [
        pltpu.make_async_copy(a, b, w_sem.at[i])
        for i, (a, b) in enumerate(((gate_hbm, gate), (up_hbm, up), (down_hbm, down)))
    ]
    for load in loads:
        load.start()

    barrier = pltpu.get_barrier_semaphore()

    def greet(k, c):
        pl.semaphore_signal(
            barrier, inc=1, device_id=(lax.rem(spi + k, n), tpi), device_id_type=MESH
        )
        return c

    lax.fori_loop(1, n, greet, 0)
    for peer in (nxt, prv, partner):
        pl.semaphore_signal(barrier, inc=1, device_id=peer, device_id_type=MESH)

    block = jnp.dot(place_ref[...], normed_ref[...], preferred_element_type=f32).astype(bf16)
    for e in range(n):
        packed[e] = block[e * SLOTS : (e + 1) * SLOTS]
    pl.semaphore_wait(barrier, n - 1 + 3)

    def to_expert(e):
        return pltpu.make_async_remote_copy(
            src_ref=packed.at[e],
            dst_ref=arrived.at[spi],
            send_sem=a_send.at[e],
            recv_sem=a_recv,
            device_id=(e, tpi),
            device_id_type=MESH,
        )

    def to_token(s):
        return pltpu.make_async_remote_copy(
            src_ref=spread.at[s],
            dst_ref=back.at[spi],
            send_sem=b_send.at[s],
            recv_sem=b_recv,
            device_id=(s, tpi),
            device_id_type=MESH,
        )

    def dispatch_body(k, c):
        to_expert(lax.rem(spi + k, n)).start()
        return c

    pltpu.make_async_copy(packed.at[spi], arrived.at[spi], a_recv).start()
    lax.fori_loop(1, n, dispatch_body, 0)

    def mine(k):
        return lax.rem(z - sign * (1 + k) + 2 * nz, nz)

    def theirs(k):
        return lax.rem(z + sign * (1 + k) + 2 * nz, nz)

    def part(s):
        return pl.ds(s * half, half)

    def ring(k, s):
        return pltpu.make_async_remote_copy(
            src_ref=xbuf.at[core, mine(k), part(s)],
            dst_ref=xbuf.at[core, mine(k), part(s)],
            send_sem=ag_send.at[k, s],
            recv_sem=ag_recv.at[lax.rem(k + 1, nz), s],
            device_id=nxt,
            device_id_type=MESH,
        )

    def share(k):
        return pltpu.make_async_remote_copy(
            src_ref=xbuf.at[core, mine(k)],
            dst_ref=xbuf.at[core, mine(k)],
            send_sem=d_send.at[k],
            recv_sem=d_recv.at[k],
            device_id=partner,
            device_id_type=MESH,
        )

    def give(k, s):
        return pltpu.make_async_remote_copy(
            src_ref=psend.at[k, part(s)],
            dst_ref=precv.at[k, part(s)],
            send_sem=p_send.at[k, s],
            recv_sem=p_recv.at[k, s],
            device_id=partner,
            device_id_type=MESH,
        )

    def reduce(k, s):
        return pltpu.make_async_remote_copy(
            src_ref=rsend.at[k, part(s)],
            dst_ref=rrecv.at[k, part(s)],
            send_sem=r_send.at[k, s],
            recv_sem=r_recv.at[k, s],
            device_id=nxt,
            device_id_type=MESH,
        )

    compact = lax.broadcasted_iota(jnp.int32, (rows, padded), 0)
    wide = lax.broadcasted_iota(jnp.int32, (rows, padded), 1)
    keep = (lax.div(compact, capacity) * SLOTS + lax.rem(compact, capacity) == wide).astype(bf16)
    pltpu.make_async_copy(arrived, arrived, a_recv).wait()
    xbuf[core, z] = jnp.dot(
        keep, arrived[...].reshape(padded, model), preferred_element_type=f32
    ).astype(bf16)
    for s in range(subs):
        ring(nz - 1, s).start()
    share(nz - 1).start()
    for load in loads:
        load.wait()

    tile = min(512, model)
    across = (((1,), (1,)), ((), ()))

    def step(k, c):
        @pl.when(k < nz - 1)
        def _():
            for s in range(subs):
                pltpu.make_async_copy(
                    xbuf.at[core, 0, part(s)], xbuf.at[core, mine(k), part(s)], ag_recv.at[k, s]
                ).wait()

                @pl.when(k < nz - 2)
                def _():
                    ring(k, s).start()

            share(k).start()

        pltpu.make_async_copy(
            xbuf.at[1 - core, 0], xbuf.at[1 - core, theirs(k)], d_recv.at[k]
        ).wait()

        x = jnp.concatenate([xbuf[1 - core, theirs(k)], xbuf[core, mine(k)]], axis=0)
        g = lax.dot_general(x, gate[...], across, preferred_element_type=f32)
        u = lax.dot_general(x, up[...], across, preferred_element_type=f32)
        hidden = (g / (1.0 + jnp.exp(-g)) * u).astype(bf16)
        for i in range(model // tile):
            cols = slice(i * tile, (i + 1) * tile)
            p = jnp.dot(hidden, down[:, cols], preferred_element_type=f32)
            psend[k, :, cols] = p[:rows].astype(bf16)
            pown[:, cols] = p[rows:]
        for s in range(subs):
            give(k, s).start()
        for s in range(subs):
            give(k, s).wait_recv()
            total = pown[part(s), :] + precv[k, part(s), :].astype(f32)

            @pl.when(k > 0)
            def _():
                kk = jnp.maximum(k - 1, 0)
                reduce(kk, s).wait_recv()
                pown[part(s), :] = total + rrecv[kk, part(s), :].astype(f32)

            @pl.when(k == 0)
            def _():
                pown[part(s), :] = total

            @pl.when(k < nz - 1)
            def _():
                rsend[k, part(s), :] = pown[part(s), :].astype(bf16)
                reduce(k, s).start()

        return c

    lax.fori_loop(0, nz, step, 0)

    finished = pown[...].astype(bf16)
    scattered = lax.dot_general(
        keep, finished, (((0,), (0,)), ((), ())), preferred_element_type=f32
    ).astype(bf16)
    for s in range(n):
        spread[s] = scattered[s * SLOTS : (s + 1) * SLOTS]
    pltpu.make_async_copy(spread.at[spi], back.at[spi], b_recv).start()

    def return_body(k, c):
        to_token(lax.rem(spi + k, n)).start()
        return c

    lax.fori_loop(1, n, return_body, 0)

    def drain(k, c):
        for s in range(subs):
            give(k, s).wait_send()

            @pl.when(k != nz - 2)
            def _():
                ring(k, s).wait_send()

            @pl.when(k < nz - 1)
            def _():
                reduce(k, s).wait_send()

        share(k).wait_send()
        return c

    lax.fori_loop(0, nz, drain, 0)

    def drain_plane(k, c):
        to_expert(lax.rem(spi + k, n)).wait_send()
        return c

    lax.fori_loop(1, n, drain_plane, 0)

    pltpu.make_async_copy(back, back, b_recv).wait()
    rows_back = back[...].reshape(padded, model)
    mixture = jnp.zeros(stream_ref.shape, f32)
    for r in range(pick_ref.shape[0]):
        picked = jnp.dot(pick_ref[r], rows_back, preferred_element_type=f32)
        mixture = mixture + picked * route_ref[:, r : r + 1]
    out_ref[...] = (stream_ref[...].astype(f32) + mixture).astype(bf16)

    def drain_back(k, c):
        to_token(lax.rem(spi + k, n)).wait_send()
        return c

    lax.fori_loop(1, n, drain_back, 0)


def experts(normed, stream, expert_ids, route_weights, gate_weight, up_weight, down_weight):
    nz = lax.axis_size("tp") // 2
    n = lax.axis_size("sp")
    tok_dev, model = normed.shape
    top = expert_ids.shape[1]
    capacity = max(2, 3 * tok_dev * top // (2 * n))
    rows = n * capacity
    padded = n * SLOTS
    inner = gate_weight.shape[2]
    bf16 = jnp.bfloat16
    flat_ids = expert_ids.reshape(-1)
    order = jnp.arange(tok_dev * top, dtype=jnp.int32)
    same = flat_ids[:, None] == flat_ids[None, :]
    rank = jnp.sum((same & (order[None, :] < order[:, None])).astype(jnp.int32), axis=1)
    slot = (flat_ids * SLOTS + rank).reshape(tok_dev, top)
    numbers = jnp.arange(padded, dtype=jnp.int32)
    place = jnp.any(numbers[:, None, None] == slot[None], axis=2).astype(bf16)
    pick = (slot.T[:, :, None] == numbers[None, None, :]).astype(bf16)
    vmem = pl.BlockSpec(memory_space=pltpu.VMEM)
    hbm = pl.BlockSpec(memory_space=pl.ANY)
    dma = pltpu.SemaphoreType.DMA
    return pl.pallas_call(
        functools.partial(experts_kernel, nz, n, capacity),
        out_shape=jax.ShapeDtypeStruct((tok_dev, model), bf16),
        in_specs=[vmem] * 5 + [hbm] * 3,
        out_specs=vmem,
        scratch_shapes=[
            pltpu.VMEM((n, SLOTS, model), bf16),
            pltpu.VMEM((n, SLOTS, model), bf16),
            pltpu.VMEM((2, nz, rows, model), bf16),
            pltpu.VMEM((inner, model), bf16),
            pltpu.VMEM((inner, model), bf16),
            pltpu.VMEM((inner, model), bf16),
            pltpu.VMEM((rows, model), jnp.float32),
            pltpu.VMEM((nz, rows, model), bf16),
            pltpu.VMEM((nz, rows, model), bf16),
            pltpu.VMEM((nz - 1, rows, model), bf16),
            pltpu.VMEM((nz - 1, rows, model), bf16),
            pltpu.VMEM((n, SLOTS, model), bf16),
            pltpu.VMEM((n, SLOTS, model), bf16),
            dma((3,)),
            dma((n,)),
            dma,
            dma((n,)),
            dma,
            dma((nz, 2)),
            dma((nz, 2)),
            dma((nz,)),
            dma((nz,)),
            dma((nz, 2)),
            dma((nz, 2)),
            dma((nz - 1, 2)),
            dma((nz - 1, 2)),
        ],
        compiler_params=pltpu.CompilerParams(
            collective_id=1, has_side_effects=True, vmem_limit_bytes=60 << 20
        ),
        name="experts",
    )(
        normed,
        stream,
        place,
        pick,
        route_weights,
        jnp.swapaxes(gate_weight[0], 0, 1),
        jnp.swapaxes(up_weight[0], 0, 1),
        down_weight[0],
    )


def shards(
    tokens,
    query_vectors,
    key_vectors,
    value_vectors,
    cum_gate,
    out_weight,
    norm_gain,
    gate_weight,
    up_weight,
    down_weight,
    expert_ids,
    route_weights,
):
    stream, normed = attention(
        query_vectors, key_vectors, value_vectors, cum_gate, out_weight, tokens, norm_gain
    )
    return experts(
        normed, stream, expert_ids, route_weights, gate_weight, up_weight, down_weight
    )


def solution(mesh):
    in_specs = (
        P(("sp", "tp"), None),
        P("sp", "tp"),
        P("sp", "tp"),
        P("sp", "tp"),
        P("sp", "tp"),
        P("tp", None),
        P(),
        P("sp", None, "tp"),
        P("sp", None, "tp"),
        P("sp", "tp", None),
        P(("sp", "tp"), None),
        P(("sp", "tp"), None),
    )
    out_specs = P(("sp", "tp"), None)
    return jax.shard_map(shards, mesh=mesh, in_specs=in_specs, out_specs=out_specs, check_vma=False)
```

time: 209 us -> 188 us (0.90)
  Pallas kernels: 136 us -> 174 us
  starting transfers between devices: 16.9 us -> 0 us
  waiting for transfers between devices: 15.5 us -> 0 us
  between operations: 13.6 us -> 0.05 us
  matrix products: 5.36 us -> 0 us
  local copies, waits for them, and re-layouts: 15.5 us -> 12 us
  other arithmetic: 4.23 us -> 1.63 us
    pallas_call x2, Pallas kernels: 136 us -> 174 us  [the longest x1 101 us: experts(): pl.pallas_call(functools.partial(experts_kernel, nz, n, capacity), out_sh...]
    all_to_all x2 -> x0, starting transfers between devices: 16.9 us -> none  [the longest x1 12.1 us: shards(): lax.all_to_all(dispatch, 'sp', split_axis=0, concat_axis=0, tiled=True)]
    all_to_all x2 -> x0, waiting for transfers between devices: 14.8 us -> none  [the longest x1 10.6 us: shards(): lax.all_to_all(returned, 'sp', split_axis=0, concat_axis=0, tiled=True)]
    dot_general x2 -> x0, matrix products: 5.36 us -> none  [the longest x1 5.12 us: shards(): jnp.dot(token_rows, lax.all_gather(out_weight, 'tp', axis=0, tiled=True),...]
    reshape x6 -> x0, local copies, waits for them, and re-layouts: 4.09 us -> none  [the longest x1 1.92 us: shards(): returned = summed.reshape(arrived.shape)]
    unnamed x16 -> x21, local copies, waits for them, and re-layouts: 7.13 us -> 11 us
    slice x3 -> x0, local copies, waits for them, and re-layouts: 2.28 us -> none  [the longest x1 1.09 us: attention(): query_vectors[:, half:]]
  transfers between devices with their start and end apart: 3 -> 0, of which waited for: 2 -> 0; matrix products, arithmetic and copies ran while one was open for 6% -> 0% of each run, Pallas kernels for 32% -> 0%
where the time goes in v3:
time: 188 us; the launch traced here: 187 us
  Pallas kernels  174 us (93%)
  local copies, waits for them, and re-layouts  12 us (6%)
    pallas_call x1, Pallas kernels, experts(): pl.pallas_call(functools.partial(experts_kernel, nz, n, capacity), out_sh...  101 us
    pallas_call x1, Pallas kernels, attention(): pl.pallas_call(functools.partial(attention_kernel, n, n_tp, coef), out_sh...  72.2 us
    unnamed x21, local copies, waits for them, and re-layouts  11 us

profile of v3, /device:TPU:2, one launch (start us, length us, event | category | flops | bytes accessed | tf_op | source)
XLA Modules:
  0.0 187.3 jit_solution(14018176831236011672)
XLA Ops:
  0.0 1.4 copy.33.route_ref
  1.4 0.8 copy.30
  2.1 0.1 eq.42
  2.2 0.2 convert_reduce_fusion
  2.4 0.1 reduce_sum.12
  2.5 0.1 copy.31
  2.6 0.7 multiply_add_fusion
  3.3 0.1 fusion
  3.4 0.7 fusion.2.pick_ref
  4.1 0.7 copy.32.place_ref
  4.8 0.0 copy-start
  4.8 1.0 copy-done
  5.8 0.0 copy-start.3
  5.8 0.9 copy-done.3
  6.7 0.0 copy-start.4
  6.7 0.9 copy-done.4
  7.6 0.0 copy-start.5
  7.6 0.9 copy-done.5
  8.5 0.0 copy-start.6
  8.5 0.9 copy-done.6
  9.4 0.0 copy-start.7
  9.4 0.7 copy-done.7
  10.1 0.0 copy-start.8
  10.1 0.7 copy-done.8
  10.8 72.2 %attention.1 = (bf16[32,2048]{1,0:T(8,128)(2,1)S(1)}, bf16[32,2048]{1,0:T(8,128)(2,1)S(1)}) custom-call(bf16[512,128]{1,0:T(8,128)(2,1)S(1)} %copy-done.3, bf16[512,128]{1,0:T(8,128)(2,1)S(1)} %copy-done.4, bf16[512,128]{1,0:T(8,128)(2,1)S(1)} %copy-done.5, f32[2,512]{1,0:T(2,128)S(1)} %bitcast.11, bf16[128,2048]{1,0:T(8,128)(2,1)S(1)} %copy-done, ...), custom_call_target="tpu_custom_call" | custom-call | tf_op jit(solution)/shard_map/attention/pallas_call | solution.py:406
  83.0 0.0 copy-start.1
  83.0 0.6 copy-done.1
  83.7 0.0 copy-start.2
  83.7 0.7 copy-done.2
  84.3 101.4 %experts.1 = bf16[32,2048]{1,0:T(8,128)(2,1)} custom-call(bf16[32,2048]{1,0:T(8,128)(2,1)} %copy-done.2, bf16[32,2048]{1,0:T(8,128)(2,1)} %copy-done.1, bf16[128,32]{1,0:T(8,128)(2,1)} %copy.32.place_ref, bf16[2,32,128]{2,1,0:T(8,128)(2,1)} %fusion.2.pick_ref, f32[32,2]{1,0:T(8,128)} %copy.33.route_ref, bf16[448,2048]{1,0:T(8,128)(2,1)} %bitcast.12, ...), custom_call_target="tpu_custom_call" | custom-call | tf_op jit(solution)/shard_map/experts/pallas_call | solution.py:750
  185.7 1.6 copy.35
  (1 shorter events, 0.0 us)
Async XLA Ops:
  4.8 1.0 copy-start
  5.8 0.9 copy-start.3
  6.7 0.9 copy-start.4
  7.6 0.9 copy-start.5
  8.5 0.9 copy-start.6
  9.4 0.7 copy-start.7
  10.1 0.7 copy-start.8
  83.0 0.7 copy-start.1
  83.7 0.7 copy-start.2

commit v4 on v1

v4 whole, which is shorter than its diff:
```python
import functools
import math

import jax
import jax.numpy as jnp
from jax import lax
from jax.experimental import pallas as pl
from jax.experimental.pallas import tpu as pltpu
from jax.sharding import PartitionSpec as P

NEG_LARGE = -1e30
MESH = pl.DeviceIdType.MESH
SLOTS = 8


def layer_kernel(
    n,
    n_tp,
    coef,
    capacity,
    q_hbm,
    k_hbm,
    v_hbm,
    gate_ref,
    w_hbm,
    tok_hbm,
    gain_ref,
    ids_ref,
    route_ref,
    wg_hbm,
    wu_hbm,
    wd_hbm,
    out_ref,
    q_ref,
    k_ref,
    v_ref,
    w_ref,
    tok_ref,
    gate,
    up,
    down,
    qraw,
    qbuf,
    kvsend,
    bsend,
    kvbuf,
    bbuf,
    peak,
    total,
    acc,
    obuf,
    rbuf,
    wbuf,
    proj,
    stream_ref,
    place,
    keep,
    ext,
    packed,
    arrived,
    xbuf,
    pown,
    psend,
    precv,
    rsend,
    rrecv,
    spread,
    back,
    in_sem,
    kv_send,
    kv_recv,
    b_send,
    b_recv,
    q_send,
    q_recv,
    o_send,
    o_recv,
    w_send,
    w_recv,
    d_send,
    d_recv,
    own_sem,
    x_send,
    x_recv,
    a_send,
    a_recv,
    s_send,
    s_recv,
    p_send,
    p_recv,
    r_send,
    r_recv,
    t_send,
    t_recv,
):
    me = lax.axis_index("sp")
    mt = lax.axis_index("tp")
    nz = n_tp // 2
    z = lax.div(mt, 2)
    core = lax.rem(mt, 2)
    sign = 1 - 2 * core
    nxt = (me, lax.rem(z + sign + nz, nz) * 2 + core)
    partner = (me, z * 2 + 1 - core)
    mirror = n - 1 - me
    head = lax.div(me, n // 2)
    pair = jnp.minimum(me, mirror)
    last = jnp.maximum(me, mirror)
    own_slot = head
    rows, width = q_ref.shape
    half = width // 2
    tok_dev, model = tok_ref.shape
    bf16, f32 = jnp.bfloat16, jnp.float32
    expert_rows = n * capacity
    padded = n * SLOTS

    loads = [
        pltpu.make_async_copy(a, b, in_sem.at[i])
        for i, (a, b) in enumerate(
            (
                (k_hbm, k_ref),
                (v_hbm, v_ref),
                (q_hbm, q_ref),
                (w_hbm, w_ref),
                (tok_hbm, tok_ref),
                (wg_hbm, gate),
                (wu_hbm, up),
                (wd_hbm, down),
            )
        )
    ]
    for load in loads:
        load.start()

    barrier = pltpu.get_barrier_semaphore()

    def greet_plane(k, c):
        pl.semaphore_signal(
            barrier, inc=1, device_id=(lax.rem(me + k, n), mt), device_id_type=MESH
        )
        return c

    def greet_heads(k, c):
        t = lax.rem(mt + k, n_tp)
        pl.semaphore_signal(barrier, inc=1, device_id=(me, t), device_id_type=MESH)
        pl.semaphore_signal(barrier, inc=1, device_id=(mirror, t), device_id_type=MESH)
        return c

    lax.fori_loop(1, n, greet_plane, 0)
    lax.fori_loop(1, n_tp, greet_heads, 0)

    own_w = pltpu.make_async_copy(w_hbm, wbuf.at[mt], own_sem.at[0])
    own_w.start()
    for load in loads[:5]:
        load.wait()
    lane = lax.broadcasted_iota(jnp.int32, (rows, width), 1)
    low = lane < half
    rolled_k = pltpu.roll(k_ref[...].astype(jnp.float32), half, 1)
    values = v_ref[...].astype(jnp.float32)
    kvsend[0] = jnp.where(low, values, rolled_k).astype(jnp.bfloat16)
    kvsend[1] = jnp.where(low, rolled_k, values).astype(jnp.bfloat16)
    bias_rows = gate_ref[...] * (-math.log2(math.e))
    bsend[0] = bias_rows[0:1]
    bsend[1] = bias_rows[1:2]
    mine = low == (head == 1)

    def prepare(raw):
        rolled = pltpu.roll(raw.astype(jnp.float32), half, 1)
        return jnp.where(mine, rolled, 0.0).astype(jnp.bfloat16)

    qbuf[own_slot] = prepare(q_ref[...])
    peak[...] = jnp.full(peak.shape, NEG_LARGE, jnp.float32)
    total[...] = jnp.zeros(total.shape, jnp.float32)
    acc[...] = jnp.zeros(acc.shape, jnp.float32)

    pl.semaphore_wait(barrier, (n - 1) + 2 * (n_tp - 1))

    q_copy = pltpu.make_async_remote_copy(
        src_ref=q_ref,
        dst_ref=qraw,
        send_sem=q_send,
        recv_sem=q_recv,
        device_id=(mirror, mt),
        device_id_type=MESH,
    )
    q_copy.start()

    w_half = w_ref.shape[0] // 2

    def w_mine(k):
        return lax.rem(z - sign * (1 + k) + 2 * nz, nz) * 2 + core

    def w_theirs(k):
        return lax.rem(z + sign * (1 + k) + 2 * nz, nz) * 2 + 1 - core

    def w_ring(k, s, src):
        return pltpu.make_async_remote_copy(
            src_ref=src.at[pl.ds(s * w_half, w_half)],
            dst_ref=wbuf.at[w_mine(k), pl.ds(s * w_half, w_half)],
            send_sem=w_send.at[k, s],
            recv_sem=w_recv.at[lax.rem(k + 1, nz), s],
            device_id=nxt,
            device_id_type=MESH,
        )

    def w_share(k, s, src):
        return pltpu.make_async_remote_copy(
            src_ref=src.at[pl.ds(s * w_half, w_half)],
            dst_ref=wbuf.at[w_mine(k), pl.ds(s * w_half, w_half)],
            send_sem=d_send.at[k, s],
            recv_sem=d_recv.at[k, s],
            device_id=partner,
            device_id_type=MESH,
        )

    for s in range(2):
        w_ring(nz - 1, s, w_ref).start()

    def kv_copy(r):
        hr = lax.div(r, n // 2)
        return (
            pltpu.make_async_remote_copy(
                src_ref=kvsend.at[hr],
                dst_ref=kvbuf.at[me],
                send_sem=kv_send.at[r],
                recv_sem=kv_recv.at[me],
                device_id=(r, mt),
                device_id_type=MESH,
            ),
            pltpu.make_async_remote_copy(
                src_ref=bsend.at[hr],
                dst_ref=bbuf.at[me],
                send_sem=b_send.at[r],
                recv_sem=b_recv.at[me],
                device_id=(r, mt),
                device_id_type=MESH,
            ),
        )

    def send_body(k, c):
        r = lax.rem(me + k, n)

        @pl.when(me <= jnp.maximum(r, n - 1 - r))
        def _():
            ck, cb = kv_copy(r)
            cb.start()
            ck.start()

        return c

    lax.fori_loop(1, n, send_body, 0)
    for s in range(2):
        w_share(nz - 1, s, w_ref).start()

    sub = min(256, rows)

    def tile(slot, kv_at, bias_at, diagonal):
        for i in range(rows // sub):
            kv = kv_at[...]
            rs = pl.ds(i * sub, sub)
            s = lax.dot_general(
                qbuf[slot, rs, :], kv, (((1,), (1,)), ((), ())), preferred_element_type=jnp.float32
            )
            s = s * coef + bias_at[...]
            if diagonal:
                qp = lax.broadcasted_iota(jnp.int32, s.shape, 0) + i * sub
                kp = lax.broadcasted_iota(jnp.int32, s.shape, 1)
                s = jnp.where(kp <= qp, s, NEG_LARGE)
            old = peak[slot, rs, :]
            new = jnp.maximum(old, jnp.max(s, axis=1, keepdims=True))
            e = jnp.exp2(s - new)
            alpha = jnp.exp2(old - new)
            total[slot, rs, :] = total[slot, rs, :] * alpha + jnp.sum(e, axis=1, keepdims=True)
            acc[slot, rs, :] = acc[slot, rs, :] * alpha + jnp.dot(
                e.astype(jnp.bfloat16), kv, preferred_element_type=jnp.float32
            )
            peak[slot, rs, :] = new

    tile(own_slot, kvsend.at[head], bsend.at[head], True)
    pltpu.make_async_copy(q_ref, qraw, q_recv).wait()
    qbuf[1 - own_slot] = prepare(qraw[...])

    @pl.when(me < last)
    def _():
        tile(1, kvsend.at[head], bsend.at[head], False)

    def w_event(i):
        k = lax.div(i, 2)
        s = lax.rem(i, 2)
        block = wbuf.at[w_mine(k)]
        pltpu.make_async_copy(
            w_ref.at[pl.ds(0, w_half)], block.at[pl.ds(s * w_half, w_half)], w_recv.at[k, s]
        ).wait()

        @pl.when(k < nz - 2)
        def _():
            w_ring(k, s, block).start()

        w_share(k, s, block).start()

    events = 2 * (nz - 1)
    early = max(0, min(events, n - 3))

    def compute_body(k, c):
        j = lax.rem(me - k + n, n)

        @pl.when(jnp.logical_and(k >= 3, k - 3 < early))
        def _():
            w_event(k - 3)

        @pl.when(j <= last)
        def _():
            pltpu.make_async_copy(kvsend.at[0], kvbuf.at[j], kv_recv.at[j]).wait()
            pltpu.make_async_copy(bsend.at[0], bbuf.at[j], b_recv.at[j]).wait()

            def slot_body(slot, c):
                end = jnp.where(slot == 0, pair, last)

                @pl.when(j == end)
                def _():
                    tile(slot, kvbuf.at[j], bbuf.at[j], True)

                @pl.when(j < end)
                def _():
                    tile(slot, kvbuf.at[j], bbuf.at[j], False)

                return c

            lax.fori_loop(0, 2, slot_body, 0)

        return c

    lax.fori_loop(1, n, compute_body, 0)

    for slot in range(2):
        obuf[slot] = (acc[slot] / total[slot]).astype(jnp.bfloat16)

    def o_target(slot):
        return jnp.where(slot == 0, pair, last)

    def o_copy(slot, t):
        return pltpu.make_async_remote_copy(
            src_ref=obuf.at[slot, pl.ds(t * tok_dev, tok_dev)],
            dst_ref=rbuf.at[mt, head],
            send_sem=o_send.at[slot, t],
            recv_sem=o_recv,
            device_id=(o_target(slot), t),
            device_id_type=MESH,
        )

    def o_self(slot, t):
        return jnp.logical_and(o_target(slot) == me, t == mt)

    def o_body(k, c):
        slot = lax.rem(k, 2)
        t = lax.rem(mt + n_tp // 2 + lax.div(k, 2), n_tp)

        @pl.when(jnp.logical_not(o_self(slot, t)))
        def _():
            o_copy(slot, t).start()

        @pl.when(o_self(slot, t))
        def _():
            pltpu.make_async_copy(
                obuf.at[slot, pl.ds(t * tok_dev, tok_dev)], rbuf.at[mt, head], o_recv
            ).start()

        return c

    lax.fori_loop(0, 2 * n_tp, o_body, 0)

    def late_event(i, c):
        w_event(i)
        return c

    lax.fori_loop(early, events, late_event, 0)

    number = lax.broadcasted_iota(jnp.int32, (n, tok_dev), 0)
    before = (
        lax.broadcasted_iota(jnp.int32, (tok_dev, tok_dev), 0)
        < lax.broadcasted_iota(jnp.int32, (tok_dev, tok_dev), 1)
    ).astype(bf16)
    expand = (
        lax.div(lax.broadcasted_iota(jnp.int32, (padded, n), 0), SLOTS)
        == lax.broadcasted_iota(jnp.int32, (padded, n), 1)
    ).astype(bf16)
    inside = lax.rem(lax.broadcasted_iota(jnp.int32, (padded, tok_dev), 0), SLOTS).astype(f32)
    taken = jnp.zeros((n, 1), f32)
    for r in range(ids_ref.shape[0]):
        named = (number == ids_ref[r : r + 1, :]).astype(f32)
        rank = jnp.dot(named.astype(bf16), before, preferred_element_type=f32) + taken
        taken = taken + jnp.sum(named, axis=1, keepdims=True)
        named_at = jnp.dot(expand, named.astype(bf16), preferred_element_type=f32)
        rank_at = jnp.dot(expand, rank.astype(bf16), preferred_element_type=f32)
        place[r] = jnp.where(rank_at == inside, named_at, 0.0).astype(bf16)
    compact = lax.broadcasted_iota(jnp.int32, (expert_rows, padded), 0)
    spaced = lax.broadcasted_iota(jnp.int32, (expert_rows, padded), 1)
    keep[...] = (
        lax.div(compact, capacity) * SLOTS + lax.rem(compact, capacity) == spaced
    ).astype(bf16)
    eye = (
        lax.broadcasted_iota(jnp.int32, (padded, padded), 0)
        == lax.broadcasted_iota(jnp.int32, (padded, padded), 1)
    ).astype(bf16)
    first = (((0,), (0,)), ((), ()))
    sent_to = place[0]
    for r in range(1, ids_ref.shape[0]):
        sent_to = sent_to + place[r]
    ext[nz - 1, :, model:] = lax.dot_general(
        sent_to, eye, first, preferred_element_type=f32
    ).astype(bf16)

    pltpu.make_async_copy(rbuf, rbuf, o_recv).wait()
    own_w.wait()
    for s in range(2):
        pltpu.make_async_copy(
            w_ref.at[pl.ds(0, w_half)], wbuf.at[mt, pl.ds(s * w_half, w_half)], d_recv.at[nz - 1, s]
        ).wait()
    low32 = lax.broadcasted_iota(jnp.int32, (tok_dev, width), 1) < half

    def product(t):
        piece = jnp.where(
            low32, rbuf[t, 0].astype(jnp.float32), rbuf[t, 1].astype(jnp.float32)
        ).astype(jnp.bfloat16)
        return jnp.dot(piece, wbuf[t], preferred_element_type=jnp.float32)

    proj[...] = product(mt)
    proj[...] += product(z * 2 + 1 - core)

    def project(k, c):
        for s in range(2):
            pltpu.make_async_copy(
                w_ref.at[pl.ds(0, w_half)],
                wbuf.at[w_theirs(k), pl.ds(s * w_half, w_half)],
                d_recv.at[k, s],
            ).wait()
        proj[...] += product(w_mine(k))
        proj[...] += product(w_theirs(k))
        return c

    lax.fori_loop(0, nz - 1, project, 0)
    stream = (tok_ref[...].astype(f32) + proj[...]).astype(bf16)
    stream_ref[...] = stream
    stream_wide = stream.astype(f32)
    inverse = lax.rsqrt(jnp.mean(stream_wide * stream_wide, axis=1, keepdims=True) + 1e-05)
    ext[nz - 1, :, :model] = (stream_wide * inverse * gain_ref[...]).astype(bf16)

    def ring(k):
        return pltpu.make_async_remote_copy(
            src_ref=ext.at[k],
            dst_ref=ext.at[lax.rem(k + 1, nz)],
            send_sem=x_send.at[k],
            recv_sem=x_recv.at[lax.rem(k + 1, nz)],
            device_id=nxt,
            device_id_type=MESH,
        )

    def to_expert(k, e):
        return pltpu.make_async_remote_copy(
            src_ref=packed.at[k, e],
            dst_ref=arrived.at[k, me],
            send_sem=a_send.at[k, e],
            recv_sem=a_recv.at[k],
            device_id=(e, mt),
            device_id_type=MESH,
        )

    def share(k):
        return pltpu.make_async_remote_copy(
            src_ref=xbuf.at[core, k],
            dst_ref=xbuf.at[core, k],
            send_sem=s_send.at[k],
            recv_sem=s_recv.at[k],
            device_id=partner,
            device_id_type=MESH,
        )

    parts = 2
    part_rows = expert_rows // parts

    def part(s):
        return pl.ds(s * part_rows, part_rows)

    def give(k, s):
        return pltpu.make_async_remote_copy(
            src_ref=psend.at[k, part(s)],
            dst_ref=precv.at[k, part(s)],
            send_sem=p_send.at[k, s],
            recv_sem=p_recv.at[k, s],
            device_id=partner,
            device_id_type=MESH,
        )

    def reduce(k, s):
        return pltpu.make_async_remote_copy(
            src_ref=rsend.at[k, part(s)],
            dst_ref=rrecv.at[k, part(s)],
            send_sem=r_send.at[k, s],
            recv_sem=r_recv.at[k, s],
            device_id=nxt,
            device_id_type=MESH,
        )

    def to_token(s):
        return pltpu.make_async_remote_copy(
            src_ref=spread.at[s],
            dst_ref=back.at[me],
            send_sem=t_send.at[s],
            recv_sem=t_recv,
            device_id=(s, mt),
            device_id_type=MESH,
        )

    def dispatch(k):
        @pl.when(k < nz - 1)
        def _():
            pltpu.make_async_copy(ext.at[0], ext.at[k], x_recv.at[k]).wait()

        @pl.when(k != nz - 2)
        def _():
            ring(k).start()

        block = lax.dot_general(
            ext[k, :, model:], ext[k, :, :model], first, preferred_element_type=f32
        ).astype(bf16)
        for e in range(n):
            packed[k, e] = block[e * SLOTS : (e + 1) * SLOTS]
        pltpu.make_async_copy(packed.at[k, me], arrived.at[k, me], a_recv.at[k]).start()

        def send(i, c):
            to_expert(k, lax.rem(me + i, n)).start()
            return c

        lax.fori_loop(1, n, send, 0)

    def first_dispatch(i, c):
        dispatch(lax.rem(i + nz - 1, nz))
        return c

    ahead = min(2, nz - 1)
    lax.fori_loop(0, ahead + 1, first_dispatch, 0)
    for load in loads[5:]:
        load.wait()

    col_tile = min(512, model)
    across = (((1,), (1,)), ((), ()))

    def step(k, c):
        @pl.when(k + ahead < nz - 1)
        def _():
            dispatch(k + ahead)

        pltpu.make_async_copy(arrived.at[k], arrived.at[k], a_recv.at[k]).wait()
        xbuf[core, k] = jnp.dot(
            keep[...], arrived[k].reshape(padded, model), preferred_element_type=f32
        ).astype(bf16)
        share(k).start()
        pltpu.make_async_copy(xbuf.at[1 - core, 0], xbuf.at[1 - core, k], s_recv.at[k]).wait()

        x = jnp.concatenate([xbuf[1 - core, k], xbuf[core, k]], axis=0)
        g = lax.dot_general(x, gate[...], across, preferred_element_type=f32)
        u = lax.dot_general(x, up[...], across, preferred_element_type=f32)
        hidden = (g / (1.0 + jnp.exp(-g)) * u).astype(bf16)
        for i in range(model // col_tile):
            cols = slice(i * col_tile, (i + 1) * col_tile)
            p = jnp.dot(hidden, down[:, cols], preferred_element_type=f32)
            psend[k, :, cols] = p[:expert_rows].astype(bf16)
            pown[:, cols] = p[expert_rows:]
        for s in range(parts):
            give(k, s).start()
        for s in range(parts):
            give(k, s).wait_recv()
            both = pown[part(s), :] + precv[k, part(s), :].astype(f32)

            @pl.when(k > 0)
            def _():
                kk = jnp.maximum(k - 1, 0)
                reduce(kk, s).wait_recv()
                pown[part(s), :] = both + rrecv[kk, part(s), :].astype(f32)

            @pl.when(k == 0)
            def _():
                pown[part(s), :] = both

            @pl.when(k < nz - 1)
            def _():
                rsend[k, part(s), :] = pown[part(s), :].astype(bf16)
                reduce(k, s).start()

        return c

    lax.fori_loop(0, nz, step, 0)

    scattered = lax.dot_general(
        keep[...], pown[...].astype(bf16), first, preferred_element_type=f32
    ).astype(bf16)
    for s in range(n):
        spread[s] = scattered[s * SLOTS : (s + 1) * SLOTS]
    pltpu.make_async_copy(spread.at[me], back.at[me], t_recv).start()

    def return_body(k, c):
        to_token(lax.rem(me + k, n)).start()
        return c

    lax.fori_loop(1, n, return_body, 0)

    q_copy.wait_send()

    def drain_body(k, c):
        r = lax.rem(me + k, n)

        @pl.when(me <= jnp.maximum(r, n - 1 - r))
        def _():
            ck, cb = kv_copy(r)
            cb.wait_send()
            ck.wait_send()

        return c

    lax.fori_loop(1, n, drain_body, 0)

    def o_drain(k, c):
        slot = lax.rem(k, 2)
        t = lax.div(k, 2)

        @pl.when(jnp.logical_not(o_self(slot, t)))
        def _():
            o_copy(slot, t).wait_send()

        return c

    lax.fori_loop(0, 2 * n_tp, o_drain, 0)

    def w_drain(k, c):
        for s in range(2):
            w_share(k, s, w_ref).wait_send()

            @pl.when(k != nz - 2)
            def _():
                w_ring(k, s, w_ref).wait_send()

        return c

    lax.fori_loop(0, nz, w_drain, 0)

    def drain(k, c):
        for s in range(parts):
            give(k, s).wait_send()

            @pl.when(k < nz - 1)
            def _():
                reduce(k, s).wait_send()

        @pl.when(k != nz - 2)
        def _():
            ring(k).wait_send()

        share(k).wait_send()

        def drain_send(i, c):
            to_expert(k, lax.rem(me + i, n)).wait_send()
            return c

        lax.fori_loop(1, n, drain_send, 0)
        return c

    lax.fori_loop(0, nz, drain, 0)

    pltpu.make_async_copy(back, back, t_recv).wait()
    rows_back = back[...].reshape(padded, model)
    diagonal = lax.broadcasted_iota(jnp.int32, (tok_dev, tok_dev), 0) == lax.broadcasted_iota(
        jnp.int32, (tok_dev, tok_dev), 1
    )
    mixture = jnp.zeros((tok_dev, model), f32)
    for r in range(ids_ref.shape[0]):
        picked = lax.dot_general(place[r], rows_back, first, preferred_element_type=f32)
        weight = jnp.sum(
            jnp.where(diagonal, route_ref[r : r + 1, :], 0.0), axis=1, keepdims=True
        )
        mixture = mixture + picked * weight
    out_ref[...] = (stream_ref[...].astype(f32) + mixture).astype(bf16)

    def drain_back(k, c):
        to_token(lax.rem(me + k, n)).wait_send()
        return c

    lax.fori_loop(1, n, drain_back, 0)


def shards(
    tokens,
    query_vectors,
    key_vectors,
    value_vectors,
    cum_gate,
    out_weight,
    norm_gain,
    gate_weight,
    up_weight,
    down_weight,
    expert_ids,
    route_weights,
):
    n = lax.axis_size("sp")
    n_tp = lax.axis_size("tp")
    nz = n_tp // 2
    rows, width = query_vectors.shape
    tok_dev, model = tokens.shape
    top = expert_ids.shape[1]
    inner = gate_weight.shape[2]
    capacity = max(2, 3 * tok_dev * top // (2 * n))
    assert capacity <= SLOTS and gate_weight.shape[0] == 1
    expert_rows = n * capacity
    padded = n * SLOTS
    coef = (width // 2) ** (-0.5) * math.log2(math.e)
    vmem = pl.BlockSpec(memory_space=pltpu.VMEM)
    hbm = pl.BlockSpec(memory_space=pl.ANY)
    bf16, f32 = jnp.bfloat16, jnp.float32
    dma = pltpu.SemaphoreType.DMA
    return pl.pallas_call(
        functools.partial(layer_kernel, n, n_tp, coef, capacity),
        out_shape=jax.ShapeDtypeStruct((tok_dev, model), bf16),
        in_specs=[hbm, hbm, hbm, vmem, hbm, hbm, vmem, vmem, vmem, hbm, hbm, hbm],
        out_specs=vmem,
        scratch_shapes=[
            pltpu.VMEM((rows, width), bf16),
            pltpu.VMEM((rows, width), bf16),
            pltpu.VMEM((rows, width), bf16),
            pltpu.VMEM((width, model), bf16),
            pltpu.VMEM((tok_dev, model), bf16),
            pltpu.VMEM((inner, model), bf16),
            pltpu.VMEM((inner, model), bf16),
            pltpu.VMEM((inner, model), bf16),
            pltpu.VMEM((rows, width), bf16),
            pltpu.VMEM((2, rows, width), bf16),
            pltpu.VMEM((2, rows, width), bf16),
            pltpu.VMEM((2, 1, rows), f32),
            pltpu.VMEM((n, rows, width), bf16),
            pltpu.VMEM((n, 1, rows), f32),
            pltpu.VMEM((2, rows, 1), f32),
            pltpu.VMEM((2, rows, 1), f32),
            pltpu.VMEM((2, rows, width), f32),
            pltpu.VMEM((2, rows, width), bf16),
            pltpu.VMEM((n_tp, 2, tok_dev, width), bf16),
            pltpu.VMEM((n_tp, width, model), bf16),
            pltpu.VMEM((tok_dev, model), f32),
            pltpu.VMEM((tok_dev, model), bf16),
            pltpu.VMEM((top, padded, tok_dev), bf16),
            pltpu.VMEM((expert_rows, padded), bf16),
            pltpu.VMEM((nz, tok_dev, model + padded), bf16),
            pltpu.VMEM((nz, n, SLOTS, model), bf16),
            pltpu.VMEM((nz, n, SLOTS, model), bf16),
            pltpu.VMEM((2, nz, expert_rows, model), bf16),
            pltpu.VMEM((expert_rows, model), f32),
            pltpu.VMEM((nz, expert_rows, model), bf16),
            pltpu.VMEM((nz, expert_rows, model), bf16),
            pltpu.VMEM((nz - 1, expert_rows, model), bf16),
            pltpu.VMEM((nz - 1, expert_rows, model), bf16),
            pltpu.VMEM((n, SLOTS, model), bf16),
            pltpu.VMEM((n, SLOTS, model), bf16),
            dma((8,)),
            dma((n,)),
            dma((n,)),
            dma((n,)),
            dma((n,)),
            dma,
            dma,
            dma((2, n_tp)),
            dma,
            dma((nz, 2)),
            dma((nz, 2)),
            dma((nz, 2)),
            dma((nz, 2)),
            dma((1,)),
            dma((nz,)),
            dma((nz,)),
            dma((nz, n)),
            dma((nz,)),
            dma((nz,)),
            dma((nz,)),
            dma((nz, 2)),
            dma((nz, 2)),
            dma((nz - 1, 2)),
            dma((nz - 1, 2)),
            dma((n,)),
            dma,
        ],
        compiler_params=pltpu.CompilerParams(
            collective_id=0, has_side_effects=True, vmem_limit_bytes=67000000
        ),
        name="layer",
    )(
        query_vectors,
        key_vectors,
        value_vectors,
        cum_gate.T,
        out_weight,
        tokens,
        norm_gain[None, :],
        expert_ids.T,
        route_weights.T,
        jnp.swapaxes(gate_weight[0], 0, 1),
        jnp.swapaxes(up_weight[0], 0, 1),
        down_weight[0],
    )


def solution(mesh):
    in_specs = (
        P(("sp", "tp"), None),
        P("sp", "tp"),
        P("sp", "tp"),
        P("sp", "tp"),
        P("sp", "tp"),
        P("tp", None),
        P(),
        P("sp", None, "tp"),
        P("sp", None, "tp"),
        P("sp", "tp", None),
        P(("sp", "tp"), None),
        P(("sp", "tp"), None),
    )
    out_specs = P(("sp", "tp"), None)
    return jax.shard_map(shards, mesh=mesh, in_specs=in_specs, out_specs=out_specs, check_vma=False)
```

time: 264 us -> 164 us (0.62)
  waiting for transfers between devices: 115 us -> 0 us
  Pallas kernels: 65.9 us -> 162 us
  matrix products: 26.4 us -> 0 us
  blocking collectives: 22.3 us -> 0 us
  between operations: 13.3 us -> 0.01 us
  local copies, waits for them, and re-layouts: 9.4 us -> 1.57 us
  starting transfers between devices: 7.56 us -> 0 us
  other arithmetic: 4.24 us -> 0 us
    pallas_call x1, Pallas kernels: 65.9 us -> 162 us  [shards(): pl.pallas_call(functools.partial(layer_kernel, n, n_tp, coef, capacity),...]
    reduce_scatter x1 -> x0, waiting for transfers between devices: 65.9 us -> none  [shards(): lax.psum_scatter(jnp.dot(hidden, down_weight[0], preferred_element_type=j...]
    all_gather x2 -> x0, waiting for transfers between devices: 39.7 us -> none  [the longest x1 39.7 us: shards(): rows_in = lax.all_gather(row_block, 'tp', axis=0, tiled=True)]
    dot_general x4 -> x0, matrix products: 26.4 us -> none  [the longest x1 13.2 us: shards(): jnp.dot(hidden, down_weight[0], preferred_element_type=jnp.float32)]
    all_to_all x1 -> x0, blocking collectives: 22.3 us -> none  [shards(): lax.all_to_all(dispatch, 'sp', split_axis=0, concat_axis=0, tiled=True)]
    all_to_all x1 -> x0, waiting for transfers between devices: 8.45 us -> none  [shards(): lax.all_to_all(returned, 'sp', split_axis=0, concat_axis=0, tiled=True)]
    all_to_all x1 -> x0, starting transfers between devices: 7.3 us -> none  [shards(): lax.all_to_all(returned, 'sp', split_axis=0, concat_axis=0, tiled=True)]
    reshape x6 -> x0, local copies, waits for them, and re-layouts: 3.27 us -> none  [the longest x1 1.92 us: shards(): returned = summed.reshape(arrived.shape)]
  transfers between devices with their start and end apart: 4 -> 0, of which waited for: 3 -> 0; matrix products, arithmetic and copies ran while one was open for 3% -> 0% of each run, Pallas kernels for 25% -> 0%
where the time goes in v4:
time: 164 us
  Pallas kernels  162 us (99%)
    pallas_call x1, Pallas kernels, shards(): pl.pallas_call(functools.partial(layer_kernel, n, n_tp, coef, capacity),...  162 us

profile of v4, /device:TPU:2, one launch (start us, length us, event | category | flops | bytes accessed | tf_op | source)
XLA Modules:
  0.0 163.7 jit_solution(2204611027539865850)
XLA Ops:
  0.0 162.2 %layer.1 = bf16[32,2048]{1,0:T(8,128)(2,1)} custom-call(bf16[512,128]{1,0:T(8,128)(2,1)} %q_hbm.1, bf16[512,128]{1,0:T(8,128)(2,1)} %k_hbm.1, bf16[512,128]{1,0:T(8,128)(2,1)} %v_hbm.1, f32[2,512]{1,0:T(2,128)} %bitcast.15, bf16[128,2048]{1,0:T(8,128)(2,1)} %w_hbm.1, bf16[32,2048]{1,0:T(8,128)(2,1)} %tok_hbm.1, f32[1,2048]{1,0:T(1,128)} %bitcast.14, ...), custom_call_target="tpu_custom_call" | custom-call | tf_op jit(solution)/shard_map/layer/pallas_call | solution.py:719
  162.2 1.6 copy.14

commit v5 on v4

--- a/solution.py
+++ b/solution.py
@@ -55,6 +55,8 @@
     stream_ref,
     place,
     keep,
+    keep_tail,
+    folds,
     ext,
     packed,
     arrived,
@@ -79,6 +81,8 @@
     w_recv,
     d_send,
     d_recv,
+    v_send,
+    v_recv,
     own_sem,
     x_send,
     x_recv,
@@ -185,6 +189,26 @@
     q_copy.start()
 
     w_half = w_ref.shape[0] // 2
+    w_sub = w_half // 2
+    w_quarter = w_half // 4
+    side = math.isqrt(n)
+    row = lax.div(me, side)
+    column = lax.rem(me, side)
+    colour = lax.rem(row + column, 2)
+    neighbours = (
+        row * side + lax.rem(column + 1, side),
+        row * side + lax.rem(column + side - 1, side),
+        lax.rem(row + 1, side) * side + column,
+        lax.rem(row + side - 1, side) * side + column,
+    )
+
+    def sub_rows(s):
+        return pl.ds(colour * w_half + s * w_sub, w_sub)
+
+    def quarter_rows(i):
+        return pl.ds(colour * w_half + i * w_quarter, w_quarter)
+
+    other_rows = pl.ds((1 - colour) * w_half, w_half)
 
     def w_mine(k):
         return lax.rem(z - sign * (1 + k) + 2 * nz, nz) * 2 + core
@@ -194,20 +218,40 @@
 
     def w_ring(k, s, src):
         return pltpu.make_async_remote_copy(
-            src_ref=src.at[pl.ds(s * w_half, w_half)],
-            dst_ref=wbuf.at[w_mine(k), pl.ds(s * w_half, w_half)],
+            src_ref=src.at[sub_rows(s)],
+            dst_ref=wbuf.at[w_mine(k), sub_rows(s)],
             send_sem=w_send.at[k, s],
             recv_sem=w_recv.at[lax.rem(k + 1, nz), s],
             device_id=nxt,
             device_id_type=MESH,
         )
 
+    def w_plane(k, i, target, src):
+        return pltpu.make_async_remote_copy(
+            src_ref=src.at[quarter_rows(i)],
+            dst_ref=wbuf.at[w_mine(k), quarter_rows(i)],
+            send_sem=v_send.at[k, i],
+            recv_sem=v_recv.at[k],
+            device_id=(target, mt),
+            device_id_type=MESH,
+        )
+
     def w_share(k, s, src):
         return pltpu.make_async_remote_copy(
-            src_ref=src.at[pl.ds(s * w_half, w_half)],
-            dst_ref=wbuf.at[w_mine(k), pl.ds(s * w_half, w_half)],
+            src_ref=src.at[sub_rows(s)],
+            dst_ref=wbuf.at[w_mine(k), sub_rows(s)],
             send_sem=d_send.at[k, s],
             recv_sem=d_recv.at[k, s],
+            device_id=partner,
+            device_id_type=MESH,
+        )
+
+    def w_share_rest(k, src):
+        return pltpu.make_async_remote_copy(
+            src_ref=src.at[other_rows],
+            dst_ref=wbuf.at[w_mine(k), other_rows],
+            send_sem=d_send.at[k, 2],
+            recv_sem=d_recv.at[k, 2],
             device_id=partner,
             device_id_type=MESH,
         )
@@ -250,6 +294,7 @@
     lax.fori_loop(1, n, send_body, 0)
     for s in range(2):
         w_share(nz - 1, s, w_ref).start()
+    w_share_rest(nz - 1, w_ref).start()
 
     sub = min(256, rows)
 
@@ -288,24 +333,44 @@
         s = lax.rem(i, 2)
         block = wbuf.at[w_mine(k)]
         pltpu.make_async_copy(
-            w_ref.at[pl.ds(0, w_half)], block.at[pl.ds(s * w_half, w_half)], w_recv.at[k, s]
+            w_ref.at[pl.ds(0, w_sub)], block.at[sub_rows(s)], w_recv.at[k, s]
         ).wait()
 
         @pl.when(k < nz - 2)
         def _():
             w_ring(k, s, block).start()
 
+        for j in range(2):
+            target = jnp.where(s == 0, neighbours[j], neighbours[2 + j])
+            w_plane(k, 2 * s + j, target, block).start()
         w_share(k, s, block).start()
 
+    def w_rest(k, c):
+        block = wbuf.at[w_mine(k)]
+        pltpu.make_async_copy(
+            w_ref.at[pl.ds(0, w_half)], block.at[other_rows], v_recv.at[k]
+        ).wait()
+        w_share_rest(k, block).start()
+        return c
+
+    def w_partner(k, t):
+        for s in range(2):
+            pltpu.make_async_copy(
+                w_ref.at[pl.ds(0, w_sub)], wbuf.at[t, sub_rows(s)], d_recv.at[k, s]
+            ).wait()
+        pltpu.make_async_copy(
+            w_ref.at[pl.ds(0, w_half)], wbuf.at[t, other_rows], d_recv.at[k, 2]
+        ).wait()
+
     events = 2 * (nz - 1)
-    early = max(0, min(events, n - 3))
+    early = max(0, min(events, n - 2))
 
     def compute_body(k, c):
         j = lax.rem(me - k + n, n)
 
-        @pl.when(jnp.logical_and(k >= 3, k - 3 < early))
-        def _():
-            w_event(k - 3)
+        @pl.when(jnp.logical_and(k >= 2, k - 2 < early))
+        def _():
+            w_event(k - 2)
 
         @pl.when(j <= last)
         def _():
@@ -373,6 +438,7 @@
         return c
 
     lax.fori_loop(early, events, late_event, 0)
+    lax.fori_loop(0, nz - 1, w_rest, 0)
 
     number = lax.broadcasted_iota(jnp.int32, (n, tok_dev), 0)
     before = (
@@ -384,6 +450,11 @@
         == lax.broadcasted_iota(jnp.int32, (padded, n), 1)
     ).astype(bf16)
     inside = lax.rem(lax.broadcasted_iota(jnp.int32, (padded, tok_dev), 0), SLOTS).astype(f32)
+    eye = (
+        lax.broadcasted_iota(jnp.int32, (padded, padded), 0)
+        == lax.broadcasted_iota(jnp.int32, (padded, padded), 1)
+    ).astype(bf16)
+    first = (((0,), (0,)), ((), ()))
     taken = jnp.zeros((n, 1), f32)
     for r in range(ids_ref.shape[0]):
         named = (number == ids_ref[r : r + 1, :]).astype(f32)
@@ -391,30 +462,42 @@
         taken = taken + jnp.sum(named, axis=1, keepdims=True)
         named_at = jnp.dot(expand, named.astype(bf16), preferred_element_type=f32)
         rank_at = jnp.dot(expand, rank.astype(bf16), preferred_element_type=f32)
-        place[r] = jnp.where(rank_at == inside, named_at, 0.0).astype(bf16)
+        placed = jnp.where(rank_at == inside, named_at, 0.0).astype(bf16)
+        place[r] = lax.dot_general(placed, eye, first, preferred_element_type=f32).astype(bf16)
     compact = lax.broadcasted_iota(jnp.int32, (expert_rows, padded), 0)
     spaced = lax.broadcasted_iota(jnp.int32, (expert_rows, padded), 1)
     keep[...] = (
         lax.div(compact, capacity) * SLOTS + lax.rem(compact, capacity) == spaced
     ).astype(bf16)
-    eye = (
-        lax.broadcasted_iota(jnp.int32, (padded, padded), 0)
-        == lax.broadcasted_iota(jnp.int32, (padded, padded), 1)
+    spare = SLOTS - capacity
+    each = capacity // spare
+    third = lax.broadcasted_iota(jnp.int32, (expert_rows, each * padded), 1)
+    kept = lax.broadcasted_iota(jnp.int32, (expert_rows, each * padded), 0)
+    kept_in = lax.rem(kept, capacity)
+    keep_tail[...] = jnp.logical_and(
+        lax.rem(third, padded)
+        == lax.div(kept, capacity) * SLOTS + capacity + lax.div(kept_in, each),
+        lax.div(third, padded) == lax.rem(kept_in, each),
     ).astype(bf16)
-    first = (((0,), (0,)), ((), ()))
+    slot = lax.broadcasted_iota(jnp.int32, (padded, each * padded), 0)
+    target = lax.broadcasted_iota(jnp.int32, (padded, each * padded), 1)
+    target_row = lax.rem(target, padded)
+    target_in = lax.rem(target_row, SLOTS)
+    folds[...] = jnp.logical_and(
+        target_in >= capacity,
+        slot
+        == lax.div(target_row, SLOTS) * SLOTS
+        + (target_in - capacity) * each
+        + lax.div(target, padded),
+    ).astype(bf16)
     sent_to = place[0]
     for r in range(1, ids_ref.shape[0]):
         sent_to = sent_to + place[r]
-    ext[nz - 1, :, model:] = lax.dot_general(
-        sent_to, eye, first, preferred_element_type=f32
-    ).astype(bf16)
+    ext[nz - 1, :, model:] = sent_to
 
     pltpu.make_async_copy(rbuf, rbuf, o_recv).wait()
     own_w.wait()
-    for s in range(2):
-        pltpu.make_async_copy(
-            w_ref.at[pl.ds(0, w_half)], wbuf.at[mt, pl.ds(s * w_half, w_half)], d_recv.at[nz - 1, s]
-        ).wait()
+    w_partner(nz - 1, z * 2 + 1 - core)
     low32 = lax.broadcasted_iota(jnp.int32, (tok_dev, width), 1) < half
 
     def product(t):
@@ -427,12 +510,7 @@
     proj[...] += product(z * 2 + 1 - core)
 
     def project(k, c):
-        for s in range(2):
-            pltpu.make_async_copy(
-                w_ref.at[pl.ds(0, w_half)],
-                wbuf.at[w_theirs(k), pl.ds(s * w_half, w_half)],
-                d_recv.at[k, s],
-            ).wait()
+        w_partner(k, w_theirs(k))
         proj[...] += product(w_mine(k))
         proj[...] += product(w_theirs(k))
         return c
@@ -510,6 +588,12 @@
             device_id_type=MESH,
         )
 
+    body = model * capacity // SLOTS
+    fold = body // each
+
+    def unfolded(flat):
+        return jnp.concatenate([flat[:, j * fold : (j + 1) * fold] for j in range(each)], axis=0)
+
     def dispatch(k):
         @pl.when(k < nz - 1)
         def _():
@@ -519,11 +603,19 @@
         def _():
             ring(k).start()
 
-        block = lax.dot_general(
-            ext[k, :, model:], ext[k, :, :model], first, preferred_element_type=f32
-        ).astype(bf16)
-        for e in range(n):
-            packed[k, e] = block[e * SLOTS : (e + 1) * SLOTS]
+        main = ext[k, :, model:]
+        tails = jnp.dot(main, folds[...], preferred_element_type=f32).astype(bf16)
+        last_columns = ext[k, :, body:model]
+        for j in range(each):
+            cols = slice(j * fold, (j + 1) * fold)
+            block = lax.dot_general(
+                jnp.concatenate([main, tails[:, j * padded : (j + 1) * padded]], axis=0),
+                jnp.concatenate([ext[k, :, cols], last_columns], axis=0),
+                first,
+                preferred_element_type=f32,
+            ).astype(bf16)
+            for e in range(n):
+                packed[k, e, :, cols] = block[e * SLOTS : (e + 1) * SLOTS]
         pltpu.make_async_copy(packed.at[k, me], arrived.at[k, me], a_recv.at[k]).start()
 
         def send(i, c):
@@ -550,8 +642,12 @@
             dispatch(k + ahead)
 
         pltpu.make_async_copy(arrived.at[k], arrived.at[k], a_recv.at[k]).wait()
-        xbuf[core, k] = jnp.dot(
-            keep[...], arrived[k].reshape(padded, model), preferred_element_type=f32
+        flat = arrived[k].reshape(padded, body)
+        xbuf[core, k, :, :body] = jnp.dot(
+            keep[...], flat, preferred_element_type=f32
+        ).astype(bf16)
+        xbuf[core, k, :, body:] = jnp.dot(
+            keep_tail[...], unfolded(flat), preferred_element_type=f32
         ).astype(bf16)
         share(k).start()
         pltpu.make_async_copy(xbuf.at[1 - core, 0], xbuf.at[1 - core, k], s_recv.at[k]).wait()
@@ -590,11 +686,16 @@
 
     lax.fori_loop(0, nz, step, 0)
 
-    scattered = lax.dot_general(
-        keep[...], pown[...].astype(bf16), first, preferred_element_type=f32
-    ).astype(bf16)
-    for s in range(n):
-        spread[s] = scattered[s * SLOTS : (s + 1) * SLOTS]
+    for j in range(each):
+        cols = slice(j * fold, (j + 1) * fold)
+        scattered = lax.dot_general(
+            jnp.concatenate([keep[...], keep_tail[:, j * padded : (j + 1) * padded]], axis=0),
+            jnp.concatenate([pown[:, cols], pown[:, body:]], axis=0).astype(bf16),
+            first,
+            preferred_element_type=f32,
+        ).astype(bf16)
+        for s in range(n):
+            spread[s, :, cols] = scattered[s * SLOTS : (s + 1) * SLOTS]
     pltpu.make_async_copy(spread.at[me], back.at[me], t_recv).start()
 
     def return_body(k, c):
@@ -638,6 +739,13 @@
             def _():
                 w_ring(k, s, w_ref).wait_send()
 
+        w_share_rest(k, w_ref).wait_send()
+
+        @pl.when(k < nz - 1)
+        def _():
+            for i in range(4):
+                w_plane(k, i, neighbours[i], w_ref).wait_send()
+
         return c
 
     lax.fori_loop(0, nz, w_drain, 0)
@@ -666,18 +774,23 @@
     lax.fori_loop(0, nz, drain, 0)
 
     pltpu.make_async_copy(back, back, t_recv).wait()
-    rows_back = back[...].reshape(padded, model)
+    rows_back = back[...].reshape(padded, body)
+    tails_back = unfolded(rows_back)
     diagonal = lax.broadcasted_iota(jnp.int32, (tok_dev, tok_dev), 0) == lax.broadcasted_iota(
         jnp.int32, (tok_dev, tok_dev), 1
     )
-    mixture = jnp.zeros((tok_dev, model), f32)
+    mixture = jnp.zeros((tok_dev, body), f32)
+    mixture_tail = jnp.zeros((tok_dev, model - body), f32)
     for r in range(ids_ref.shape[0]):
-        picked = lax.dot_general(place[r], rows_back, first, preferred_element_type=f32)
+        chosen = place[r]
+        tails = jnp.dot(chosen, folds[...], preferred_element_type=f32).astype(bf16)
         weight = jnp.sum(
             jnp.where(diagonal, route_ref[r : r + 1, :], 0.0), axis=1, keepdims=True
         )
-        mixture = mixture + picked * weight
-    out_ref[...] = (stream_ref[...].astype(f32) + mixture).astype(bf16)
+        mixture += weight * jnp.dot(chosen, rows_back, preferred_element_type=f32)
+        mixture_tail += weight * jnp.dot(tails, tails_back, preferred_element_type=f32)
+    out_ref[:, :body] = (stream_ref[:, :body].astype(f32) + mixture).astype(bf16)
+    out_ref[:, body:] = (stream_ref[:, body:].astype(f32) + mixture_tail).astype(bf16)
 
     def drain_back(k, c):
         to_token(lax.rem(me + k, n)).wait_send()
@@ -708,7 +821,9 @@
     top = expert_ids.shape[1]
     inner = gate_weight.shape[2]
     capacity = max(2, 3 * tok_dev * top // (2 * n))
-    assert capacity <= SLOTS and gate_weight.shape[0] == 1
+    assert capacity < SLOTS and capacity % (SLOTS - capacity) == 0 and gate_weight.shape[0] == 1
+    each = capacity // (SLOTS - capacity)
+    body = model * capacity // SLOTS
     expert_rows = n * capacity
     padded = n * SLOTS
     coef = (width // 2) ** (-0.5) * math.log2(math.e)
@@ -744,19 +859,21 @@
             pltpu.VMEM((n_tp, width, model), bf16),
             pltpu.VMEM((tok_dev, model), f32),
             pltpu.VMEM((tok_dev, model), bf16),
-            pltpu.VMEM((top, padded, tok_dev), bf16),
+            pltpu.VMEM((top, tok_dev, padded), bf16),
             pltpu.VMEM((expert_rows, padded), bf16),
+            pltpu.VMEM((expert_rows, each * padded), bf16),
+            pltpu.VMEM((padded, each * padded), bf16),
             pltpu.VMEM((nz, tok_dev, model + padded), bf16),
-            pltpu.VMEM((nz, n, SLOTS, model), bf16),
-            pltpu.VMEM((nz, n, SLOTS, model), bf16),
+            pltpu.VMEM((nz, n, SLOTS, body), bf16),
+            pltpu.VMEM((nz, n, SLOTS, body), bf16),
             pltpu.VMEM((2, nz, expert_rows, model), bf16),
             pltpu.VMEM((expert_rows, model), f32),
             pltpu.VMEM((nz, expert_rows, model), bf16),
             pltpu.VMEM((nz, expert_rows, model), bf16),
             pltpu.VMEM((nz - 1, expert_rows, model), bf16),
             pltpu.VMEM((nz - 1, expert_rows, model), bf16),
-            pltpu.VMEM((n, SLOTS, model), bf16),
-            pltpu.VMEM((n, SLOTS, model), bf16),
+            pltpu.VMEM((n, SLOTS, body), bf16),
+            pltpu.VMEM((n, SLOTS, body), bf16),
             dma((8,)),
             dma((n,)),
             dma((n,)),
@@ -768,8 +885,10 @@
             dma,
             dma((nz, 2)),
             dma((nz, 2)),
-            dma((nz, 2)),
-            dma((nz, 2)),
+            dma((nz, 3)),
+            dma((nz, 3)),
+            dma((nz - 1, 4)),
+            dma((nz - 1,)),
             dma((1,)),
             dma((nz,)),
             dma((nz,)),

time: 164 us -> 152 us (0.927)
  Pallas kernels: 162 us -> 151 us
    pallas_call x1, Pallas kernels: 162 us -> 151 us  [shards(): pl.pallas_call(functools.partial(layer_kernel, n, n_tp, coef, capacity),...]
where the time goes in v5:
time: 152 us
  Pallas kernels  151 us (99%)
  local copies, waits for them, and re-layouts  1.57 us (1%)
    pallas_call x1, Pallas kernels, shards(): pl.pallas_call(functools.partial(layer_kernel, n, n_tp, coef, capacity),...  151 us

profile of v5, /device:TPU:2, one launch (start us, length us, event | category | flops | bytes accessed | tf_op | source)
XLA Modules:
  0.0 152.2 jit_solution(7862554050381823749)
XLA Ops:
  0.0 150.6 %layer.1 = bf16[32,2048]{1,0:T(8,128)(2,1)} custom-call(bf16[512,128]{1,0:T(8,128)(2,1)} %q_hbm.1, bf16[512,128]{1,0:T(8,128)(2,1)} %k_hbm.1, bf16[512,128]{1,0:T(8,128)(2,1)} %v_hbm.1, f32[2,512]{1,0:T(2,128)} %bitcast.15, bf16[128,2048]{1,0:T(8,128)(2,1)} %w_hbm.1, bf16[32,2048]{1,0:T(8,128)(2,1)} %tok_hbm.1, f32[1,2048]{1,0:T(1,128)} %bitcast.14, ...), custom_call_target="tpu_custom_call" | custom-call | tf_op jit(solution)/shard_map/layer/pallas_call | solution.py:834
  150.6 1.6 %copy.14 = bf16[32,2048]{1,0:T(8,128)(2,1)} copy(bf16[32,2048]{1,0:T(8,128)(2,1)} %layer.1) | data formatting | bytes 262144

commit v6 on v5

--- a/solution.py
+++ b/solution.py
@@ -628,7 +628,7 @@
         dispatch(lax.rem(i + nz - 1, nz))
         return c
 
-    ahead = min(2, nz - 1)
+    ahead = min(3, nz - 1)
     lax.fori_loop(0, ahead + 1, first_dispatch, 0)
     for load in loads[5:]:
         load.wait()
@@ -636,11 +636,7 @@
     col_tile = min(512, model)
     across = (((1,), (1,)), ((), ()))
 
-    def step(k, c):
-        @pl.when(k + ahead < nz - 1)
-        def _():
-            dispatch(k + ahead)
-
+    def gather(k):
         pltpu.make_async_copy(arrived.at[k], arrived.at[k], a_recv.at[k]).wait()
         flat = arrived[k].reshape(padded, body)
         xbuf[core, k, :, :body] = jnp.dot(
@@ -650,6 +646,10 @@
             keep_tail[...], unfolded(flat), preferred_element_type=f32
         ).astype(bf16)
         share(k).start()
+
+    gather(0)
+
+    def step(k, c):
         pltpu.make_async_copy(xbuf.at[1 - core, 0], xbuf.at[1 - core, k], s_recv.at[k]).wait()
 
         x = jnp.concatenate([xbuf[1 - core, k], xbuf[core, k]], axis=0)
@@ -663,6 +663,15 @@
             pown[:, cols] = p[expert_rows:]
         for s in range(parts):
             give(k, s).start()
+
+        @pl.when(k + ahead < nz - 1)
+        def _():
+            dispatch(k + ahead)
+
+        @pl.when(k < nz - 1)
+        def _():
+            gather(k + 1)
+
         for s in range(parts):
             give(k, s).wait_recv()
             both = pown[part(s), :] + precv[k, part(s), :].astype(f32)

time: 152 us -> 145 us (0.954)
  Pallas kernels: 151 us -> 143 us
    pallas_call x1, Pallas kernels: 151 us -> 143 us  [shards(): pl.pallas_call(functools.partial(layer_kernel, n, n_tp, coef, capacity),...]
where the time goes in v6:
time: 145 us
  Pallas kernels  143 us (99%)
  local copies, waits for them, and re-layouts  1.57 us (1%)
    pallas_call x1, Pallas kernels, shards(): pl.pallas_call(functools.partial(layer_kernel, n, n_tp, coef, capacity),...  143 us

profile of v6, /device:TPU:2, one launch (start us, length us, event | category | flops | bytes accessed | tf_op | source)
XLA Modules:
  0.0 144.8 jit_solution(12202091099663909362)
XLA Ops:
  0.0 143.2 %layer.1 = bf16[32,2048]{1,0:T(8,128)(2,1)} custom-call(bf16[512,128]{1,0:T(8,128)(2,1)} %q_hbm.1, bf16[512,128]{1,0:T(8,128)(2,1)} %k_hbm.1, bf16[512,128]{1,0:T(8,128)(2,1)} %v_hbm.1, f32[2,512]{1,0:T(2,128)} %bitcast.15, bf16[128,2048]{1,0:T(8,128)(2,1)} %w_hbm.1, bf16[32,2048]{1,0:T(8,128)(2,1)} %tok_hbm.1, f32[1,2048]{1,0:T(1,128)} %bitcast.14, ...), custom_call_target="tpu_custom_call" | custom-call | tf_op jit(solution)/shard_map/layer/pallas_call | solution.py:843
  143.3 1.6 %copy.14 = bf16[32,2048]{1,0:T(8,128)(2,1)} copy(bf16[32,2048]{1,0:T(8,128)(2,1)} %layer.1) | data formatting | bytes 262144

commit v7 on v6

--- a/solution.py
+++ b/solution.py
@@ -51,6 +51,7 @@
     obuf,
     rbuf,
     wbuf,
+    attended,
     proj,
     stream_ref,
     place,
@@ -340,10 +341,15 @@
         def _():
             w_ring(k, s, block).start()
 
+        w_share(k, s, block).start()
+
+    def w_pass(i, c):
+        k = lax.div(i, 2)
+        s = lax.rem(i, 2)
         for j in range(2):
             target = jnp.where(s == 0, neighbours[j], neighbours[2 + j])
-            w_plane(k, 2 * s + j, target, block).start()
-        w_share(k, s, block).start()
+            w_plane(k, 2 * s + j, target, wbuf.at[w_mine(k)]).start()
+        return c
 
     def w_rest(k, c):
         block = wbuf.at[w_mine(k)]
@@ -363,14 +369,19 @@
         ).wait()
 
     events = 2 * (nz - 1)
-    early = max(0, min(events, n - 2))
+    early = max(0, min(events, n - 1))
+    passed = early
 
     def compute_body(k, c):
         j = lax.rem(me - k + n, n)
 
-        @pl.when(jnp.logical_and(k >= 2, k - 2 < early))
-        def _():
-            w_event(k - 2)
+        @pl.when(k - 1 < early)
+        def _():
+            w_event(k - 1)
+
+        @pl.when(k - 1 < early)
+        def _():
+            w_pass(k - 1, 0)
 
         @pl.when(j <= last)
         def _():
@@ -438,6 +449,7 @@
         return c
 
     lax.fori_loop(early, events, late_event, 0)
+    lax.fori_loop(passed, events, w_pass, 0)
     lax.fori_loop(0, nz - 1, w_rest, 0)
 
     number = lax.broadcasted_iota(jnp.int32, (n, tok_dev), 0)
@@ -500,22 +512,26 @@
     w_partner(nz - 1, z * 2 + 1 - core)
     low32 = lax.broadcasted_iota(jnp.int32, (tok_dev, width), 1) < half
 
-    def product(t):
-        piece = jnp.where(
-            low32, rbuf[t, 0].astype(jnp.float32), rbuf[t, 1].astype(jnp.float32)
-        ).astype(jnp.bfloat16)
-        return jnp.dot(piece, wbuf[t], preferred_element_type=jnp.float32)
-
-    proj[...] = product(mt)
-    proj[...] += product(z * 2 + 1 - core)
-
-    def project(k, c):
+    def w_arrived(k, c):
         w_partner(k, w_theirs(k))
-        proj[...] += product(w_mine(k))
-        proj[...] += product(w_theirs(k))
-        return c
-
-    lax.fori_loop(0, nz - 1, project, 0)
+        return c
+
+    lax.fori_loop(0, nz - 1, w_arrived, 0)
+    for t in range(n_tp):
+        attended[:, t * width : (t + 1) * width] = jnp.where(
+            low32, rbuf[t, 0].astype(f32), rbuf[t, 1].astype(f32)
+        ).astype(bf16)
+    out_tile = min(512, model)
+    for i in range(model // out_tile):
+        cols = slice(i * out_tile, (i + 1) * out_tile)
+        sums = jnp.zeros((tok_dev, out_tile), f32)
+        for t in range(0, n_tp, 2):
+            sums += jnp.dot(
+                attended[:, t * width : (t + 2) * width],
+                wbuf[t : t + 2, :, cols].reshape(2 * width, out_tile),
+                preferred_element_type=f32,
+            )
+        proj[:, cols] = sums
     stream = (tok_ref[...].astype(f32) + proj[...]).astype(bf16)
     stream_ref[...] = stream
     stream_wide = stream.astype(f32)
@@ -552,7 +568,7 @@
             device_id_type=MESH,
         )
 
-    parts = 2
+    parts = 3
     part_rows = expert_rows // parts
 
     def part(s):
@@ -866,6 +882,7 @@
             pltpu.VMEM((2, rows, width), bf16),
             pltpu.VMEM((n_tp, 2, tok_dev, width), bf16),
             pltpu.VMEM((n_tp, width, model), bf16),
+            pltpu.VMEM((tok_dev, model), bf16),
             pltpu.VMEM((tok_dev, model), f32),
             pltpu.VMEM((tok_dev, model), bf16),
             pltpu.VMEM((top, tok_dev, padded), bf16),
@@ -905,10 +922,10 @@
             dma((nz,)),
             dma((nz,)),
             dma((nz,)),
-            dma((nz, 2)),
-            dma((nz, 2)),
-            dma((nz - 1, 2)),
-            dma((nz - 1, 2)),
+            dma((nz, 3)),
+            dma((nz, 3)),
+            dma((nz - 1, 3)),
+            dma((nz - 1, 3)),
             dma((n,)),
             dma,
         ],

time: 145 us -> 142 us (0.979)
  Pallas kernels: 143 us -> 140 us
    pallas_call x1, Pallas kernels: 143 us -> 140 us  [shards(): pl.pallas_call(functools.partial(layer_kernel, n, n_tp, coef, capacity),...]
where the time goes in v7:
time: 142 us; the launch traced here: 141 us
  Pallas kernels  140 us (99%)
  local copies, waits for them, and re-layouts  1.57 us (1%)
    pallas_call x1, Pallas kernels, shards(): pl.pallas_call(functools.partial(layer_kernel, n, n_tp, coef, capacity),...  140 us

profile of v7, /device:TPU:2, one launch (start us, length us, event | category | flops | bytes accessed | tf_op | source)
XLA Modules:
  0.0 141.3 jit_solution(5293499434011523640)
XLA Ops:
  0.0 139.7 %layer.1 = bf16[32,2048]{1,0:T(8,128)(2,1)} custom-call(bf16[512,128]{1,0:T(8,128)(2,1)} %q_hbm.1, bf16[512,128]{1,0:T(8,128)(2,1)} %k_hbm.1, bf16[512,128]{1,0:T(8,128)(2,1)} %v_hbm.1, f32[2,512]{1,0:T(2,128)} %bitcast.15, bf16[128,2048]{1,0:T(8,128)(2,1)} %w_hbm.1, bf16[32,2048]{1,0:T(8,128)(2,1)} %tok_hbm.1, f32[1,2048]{1,0:T(1,128)} %bitcast.14, ...), custom_call_target="tpu_custom_call" | custom-call | tf_op jit(solution)/shard_map/layer/pallas_call | solution.py:859
  139.7 1.6 %copy.14 = bf16[32,2048]{1,0:T(8,128)(2,1)} copy(bf16[32,2048]{1,0:T(8,128)(2,1)} %layer.1) | data formatting | bytes 262144
